TPU v7x, 512 devices: a 8x2x16 block of a 8x8x16 slice. The times are simulated.
512 devices in a mesh: grp: 2 (over y), ep: 32 (over z, core), tp: 8 (over x).
Axes of the slice: x: 8, y: 2, z: 16, core: 2. Of those that a mesh axis runs over, the one named last changes fastest.
The devices are a block of a 8x8x16 slice.
Arguments:
- tokens: bfloat16 [4096, 2048], P(('grp', 'ep')), parts along dimension 0, may hold values from -6 to 6
- norm_gain: float32 [2048], replicated, may hold values from 0.1 to 1.9
- routes: int32 [4096, 6], P(('grp', 'ep')), parts along dimension 0, may hold values from 0 to 31, all different within a row; in each aligned block of 64 rows (0 to 63, 64 to 127, ...) at most 24 rows name the same one
- route_weights: float32 [4096, 6], P(('grp', 'ep')), parts along dimension 0, may hold values from 0.05 to 1
- w_gate: bfloat16 [32, 2048, 2048], P('ep', None, 'tp'), may hold values from -0.125 to 0.125
- w_up: bfloat16 [32, 2048, 2048], P('ep', None, 'tp'), may hold values from -0.125 to 0.125
- w_down: bfloat16 [32, 2048, 2048], P('ep', 'tp'), may hold values from -4 to 4
- final_gain: float32 [2048], P('tp'), may hold values from 0.1 to 1.9
Outputs:
- mixed_out: bfloat16 [4096, 2048], P(('grp', 'ep'), 'tp'), parts along dimension 0
There are 2 independent parts, one for each index of `grp`. A program takes and returns all parts, laid end to end along the dimension named above; an argument that names none is the same for every part. Nothing has to cross between parts.
Inputs may be any that keep to these rules, and one draw needn't show every extreme that they name: `routes`: each row names 6 different experts; within the rows of one index of ep no expert is named by more than 24 rows, and in every draw some expert is named by exactly 24 rows of some index.
All inputs are finite; a program needn't handle non-finite values.
Results may differ from a plain program's by a relative error of at most 0.015.
Values may be sent and summed in bfloat16 or wider, within the bound.
A program may use at most 64 MiB of HBM per device.

v0:
```python
import jax
import jax.numpy as jnp
from jax import lax
from jax.sharding import PartitionSpec as P

TOP_K = 6


EPS = 1e-06


def split_up(shard, dim, count):
    before, after = (shard.shape[:dim], shard.shape[dim + 1 :])
    return jnp.moveaxis(shard.reshape(*before, count, -1, *after), dim, 0)


def sum_at_owner(shard, axis, dim):
    parts = split_up(shard, dim, lax.axis_size(axis))
    arrived = lax.all_to_all(parts, axis, split_axis=0, concat_axis=0, tiled=True)
    return arrived.astype(jnp.float32).sum(axis=0)


def copy_for_each(shard, axis):
    count = lax.axis_size(axis)
    return lax.all_to_all(
        jnp.broadcast_to(shard[None], (count, *shard.shape)), axis, 0, 0, tiled=True
    )


def taken_together(shard, axis):
    return copy_for_each(shard, axis).sum(axis=0)


def slot_table(route_rows, experts_all, capacity):
    flattened = route_rows.reshape(-1)
    matches = (flattened[:, None] == jnp.arange(experts_all, dtype=jnp.int32)[None, :]).astype(
        jnp.int32
    )
    earlier = jnp.cumsum(matches, axis=0) - matches
    slot_of = jnp.sum(earlier * matches, axis=1)
    return (flattened * capacity + slot_of).reshape(route_rows.shape)


def per_device(tokens, norm_gain, routes, route_weights, w_gate, w_up, w_down, final_gain):
    tok_count, features = tokens.shape
    ep_size = lax.axis_size("ep")
    tp_size = lax.axis_size("tp")
    exp_local = w_gate.shape[0]
    experts_all = exp_local * ep_size
    capacity = max(2, min(tok_count, 2 * tok_count * TOP_K // experts_all))
    slot_count = experts_all * capacity
    tokens_f = tokens.astype(jnp.float32)
    inverse = lax.rsqrt(jnp.mean(tokens_f * tokens_f, axis=1, keepdims=True) + EPS)
    normed = (tokens_f * inverse * norm_gain[None, :]).astype(jnp.bfloat16)
    places = slot_table(routes, experts_all, capacity)
    slot_ids = jnp.arange(slot_count, dtype=jnp.int32)
    matched = places[:, :, None] == slot_ids[None, None, :]
    selector = jnp.sum(matched.astype(jnp.float32), axis=1).T.astype(jnp.bfloat16)
    combine_rows = jnp.sum(jnp.where(matched, route_weights[:, :, None], 0.0), axis=1)
    col_share = features // tp_size
    columns = lax.dynamic_slice_in_dim(normed, lax.axis_index("tp") * col_share, col_share, 1)
    outgoing = jnp.dot(selector, columns, preferred_element_type=jnp.float32).astype(jnp.bfloat16)
    outgoing = outgoing.reshape(ep_size, exp_local, capacity, col_share)
    piece = lax.all_gather(
        lax.all_to_all(outgoing, "ep", split_axis=0, concat_axis=0, tiled=True),
        "tp",
        axis=3,
        tiled=True,
    )
    gate_part = jnp.einsum("secd,edf->secf", piece, w_gate, preferred_element_type=jnp.float32)
    up_part = jnp.einsum("secd,edf->secf", piece, w_up, preferred_element_type=jnp.float32)
    hidden = (jax.nn.silu(gate_part) * up_part).astype(jnp.bfloat16)
    partial_value = jnp.einsum("secf,efd->secd", hidden, w_down, preferred_element_type=jnp.float32)
    summed = sum_at_owner(partial_value.astype(jnp.bfloat16), "tp", 3).astype(jnp.bfloat16)
    returned = lax.all_to_all(summed, "ep", split_axis=0, concat_axis=0, tiled=True)
    results = returned.reshape(slot_count, returned.shape[3]).astype(jnp.float32)
    combined = jnp.dot(combine_rows, results)
    local_squares = jnp.sum(combined * combined, axis=1)
    squares_all = taken_together(local_squares, "tp")
    inverse_out = lax.rsqrt(squares_all / features + EPS)
    return (combined * inverse_out[:, None] * final_gain[None, :]).astype(jnp.bfloat16)


def solution(mesh):
    placed = (
        P(("grp", "ep"), None),
        P(),
        P(("grp", "ep"), None),
        P(("grp", "ep"), None),
        P("ep", None, "tp"),
        P("ep", None, "tp"),
        P("ep", "tp", None),
        P("tp"),
    )
    return jax.shard_map(
        per_device, mesh=mesh, in_specs=placed, out_specs=P(("grp", "ep"), "tp"), check_vma=False
    )
```

profile of v0, /device:TPU:65, one launch (start us, length us, event | category | flops | bytes accessed | tf_op | source)
XLA Modules:
  0.0 288.1 jit_solution(13388018511111582806)
XLA Ops:
  6.5 0.0 copy-start
  6.6 0.0 all-gather.2.cloned.1.call-start
  6.6 0.9 copy.45
  7.5 0.1 eq.42
  7.6 0.1 eq.38
  7.8 1.1 multiply_reduce_fusion
  8.9 1.0 convert_element_type.48
  9.9 0.9 reduce-window.6
  10.8 0.2 slice_reduce_fusion
  11.0 0.1 fusion.36
  11.1 0.1 reduce_sum.71
  11.3 0.1 copy.48
  11.4 0.7 multiply_add_fusion
  12.1 0.8 dynamic-slice
  12.8 1.0 convert_reduce_fusion
  13.8 0.3 convolution_convert_fusion.1
  14.1 72.6 %all_to_all.21 = bf16[32,1,24,256]{3,2,1,0:T(8,128)(2,1)} all-to-all(bf16[32,1,24,256]{3,2,1,0:T(8,128)(2,1)S(1)} %bitcast.99), channel_id=1, replica_groups=mesh['grp'=2,'ep'=32,'tp'=8] {'ep'}, dimensions={0} | all-to-all | bytes 786432 | tf_op jit(solution)/shard_map/all_to_all | solution.py:65
  86.7 0.1 all-gather.2.cloned.1.call-update
  86.8 50.0 %all-gather.2.cloned.1.call-done = bf16[32,1,24,2048]{3,2,0,1:T(8,128)(2,1)} async-done(((bf16[32,1,24,256]{3,2,0,1:T(8,128)(2,1)}), bf16[32,1,24,2048]{3,2,0,1:T(8,128)(2,1)}) %all-gather.2.cloned.1.call-update) | async-done | bytes 3145744 | tf_op jit(solution)/shard_map/all_gather | solution.py:64
  136.8 0.0 copy-done.2
  136.8 3.8 %fusion.4 = f32[32,1,24,256]{3,2,0,1:T(8,128)} fusion(bf16[32,1,24,2048]{3,2,0,1:T(8,128)(2,1)} %all-gather.2.cloned.1.call-done, bf16[1,2048,256]{2,1,0:T(8,128)(2,1)S(1)} %copy-done.2), kind=kOutput, calls=%fused_computation.6 | convolution fusion | flops 805306368 | bytes 4980736 | tf_op jit(solution)/shard_map/secd,edf->secf/dot_general | solution.py:70
  140.6 0.0 copy-done
  140.6 0.0 copy-done.3
  140.6 7.2 %convolution_convert_fusion = bf16[32,24,2048]{2,1,0:T(8,128)(2,1)} fusion(bf16[32,1,24,2048]{3,2,0,1:T(8,128)(2,1)} %all-gather.2.cloned.1.call-done, bf16[1,256,2048]{2,1,0:T(8,128)(2,1)S(1)} %copy-done, bf16[1,2048,256]{2,1,0:T(8,128)(2,1)S(1)} %copy-done.3, f32[32,1,24,256]{3,2,0,1:T(8,128)} %fusion.4), kind=kOutput, calls=%fused_computation | convolution fusion | flops 1613365248 | bytes 9175040 | tf_op jit(solution)/shard_map/secf,efd->secd/dot_general | solution.py:73
  147.8 2.1 copy.57
  149.9 72.2 %all_to_all.22 = bf16[8,32,1,24,256]{4,3,1,2,0:T(8,128)(2,1)} all-to-all(bf16[8,32,1,24,256]{4,3,1,2,0:T(8,128)(2,1)S(1)} %bitcast.96), channel_id=1, replica_groups=mesh['grp'=2,'ep'=32,'tp'=8] {'tp'}, dimensions={0} | all-to-all | bytes 6291456 | tf_op jit(solution)/shard_map/all_to_all | solution.py:19
  222.1 2.5 reduce_sum.75
  224.6 46.6 %all_to_all.23 = bf16[32,1,24,256]{3,2,1,0:T(8,128)(2,1)S(1)} all-to-all(bf16[32,1,24,256]{3,2,1,0:T(8,128)(2,1)S(1)} %bitcast.101), channel_id=1, replica_groups=mesh['grp'=2,'ep'=32,'tp'=8] {'ep'}, dimensions={0} | all-to-all | bytes 786432 | tf_op jit(solution)/shard_map/all_to_all | solution.py:75
  271.2 0.3 multiply_reduce_fusion.1
  271.5 9.0 %all_to_all.24 = f32[8,1,64]{2,1,0:T(1,128)S(1)} all-to-all(f32[8,1,64]{2,1,0:T(1,128)S(1)} %broadcast_in_dim.16), channel_id=1, replica_groups=mesh['grp'=2,'ep'=32,'tp'=8] {'tp'}, dimensions={0} | all-to-all | bytes 4096 | tf_op jit(solution)/shard_map/all_to_all | solution.py:25
  280.5 0.0 copy-done.1
  280.5 0.7 multiply_convert_fusion
  (9 shorter events, 0.1 us)
Async XLA Ops:
  6.5 134.0 %copy-start = (bf16[1,256,2048]{2,1,0:T(8,128)(2,1)S(1)}, bf16[1,256,2048]{2,1,0:T(8,128)(2,1)}, u32[]{:S(2)}) copy-start(bf16[1,256,2048]{2,1,0:T(8,128)(2,1)} %param.14) | copy-start | bytes 3145732
  6.6 130.3 %copy-start.2 = (bf16[1,2048,256]{2,1,0:T(8,128)(2,1)S(1)}, bf16[1,2048,256]{2,1,0:T(8,128)(2,1)}, u32[]{:S(2)}) copy-start(bf16[1,2048,256]{2,1,0:T(8,128)(2,1)} %param.12) | copy-start | bytes 3145732
  6.6 130.3 %all-gather.2.cloned.1.call-start = ((), (), s32[]{:S(2)}) async-start(), calls=%async_computation.4 | async-start | bytes 3538944 | tf_op jit(solution)/shard_map/all_gather | solution.py:64
  86.7 53.9 %copy-start.3 = (bf16[1,2048,256]{2,1,0:T(8,128)(2,1)S(1)}, bf16[1,2048,256]{2,1,0:T(8,128)(2,1)}, u32[]{:S(2)}) copy-start(bf16[1,2048,256]{2,1,0:T(8,128)(2,1)} %param.13) | copy-start | bytes 3145732
  222.1 58.4 %copy-start.1 = (f32[256]{0:T(256)S(1)}, f32[256]{0:T(256)}, u32[]{:S(2)}) copy-start(f32[256]{0:T(256)} %param.15) | copy-start | bytes 3076
Sparse Core Ops, SparseCore 0:
  86.9 49.8 all-gather.1
where the time goes:
time: 289 us; the launch traced here: 288 us
  blocking collectives  200 us (69%)
  waiting for transfers between devices  50.1 us (17%)
  between operations  13.5 us (5%)
  matrix products  11.6 us (4%)
  other arithmetic  8.04 us (3%)
  local copies, waits for them, and re-layouts  4.5 us (2%)
    all_to_all x1, blocking collectives, per_device(): lax.all_to_all(outgoing, 'ep', split_axis=0, concat_axis=0, tiled=True)  72.6 us
    all_to_all x1, blocking collectives, sum_at_owner(): lax.all_to_all(parts, axis, split_axis=0, concat_axis=0, tiled=True)  72.2 us
    all_gather x1, waiting for transfers between devices, per_device(): lax.all_gather(lax.all_to_all(outgoing, 'ep', split_axis=0, concat_axis=0...  50 us
    all_to_all x1, blocking collectives, per_device(): lax.all_to_all(summed, 'ep', split_axis=0, concat_axis=0, tiled=True)  46.6 us
    all_to_all x1, blocking collectives, copy_for_each(): lax.all_to_all(jnp.broadcast_to(shard[None], (count, *shard.shape)), axis...  8.97 us
    dot_general x1, matrix products, per_device(): jnp.einsum('secf,efd->secd', hidden, w_down, preferred_element_type=jnp.f...  7.17 us
  transfers between devices with their start and end apart: 1, of which 1 were waited for; matrix products, arithmetic and copies ran while one was open for 0% of the time, Pallas kernels for 0%

commit v1 on v0

v1 whole, which is shorter than its diff:
```python
import functools

import jax
import jax.numpy as jnp
from jax import lax
from jax.experimental import pallas as pl
from jax.experimental.pallas import tpu as pltpu
from jax.sharding import PartitionSpec as P

TOP_K = 6
EPS = 1e-06
MESH = pl.DeviceIdType.MESH
BF16, F32, I32 = jnp.bfloat16, jnp.float32, jnp.int32
CORES = 2


def wrap(value, count):
    return lax.rem(value + 4 * count, count)


def kernel(
    ep, tp, cap,
    tokens, norm_gain, routes, route_weights, w_gate, w_up, w_down, final_gain,
    out,
    tok, tab, rows, part, rs_long, rs_short, ret, results, squares,
    tok_in, gain_in, routes_in, weights_in, wgu, wd, final_in, c_hi, c_lo,
    in_sem, z_send, z_recv, d_send, d_recv, x_send, x_recv, l_send, l_recv, s_send, s_recv,
    r_send, r_recv, q_send, q_recv,
):
    e = lax.axis_index("ep")
    x = lax.axis_index("tp")
    z, c = lax.div(e, CORES), lax.rem(e, CORES)
    nz = ep // CORES
    steps = nz // 2
    zs = tp - 2
    back = tp // 2 - 2
    hl, hs = tp // 2, tp - 1 - tp // 2
    blk = tok_in.shape[1]
    share = tok_in.shape[2]
    last = steps - 1
    half = zs // 2

    def dev(zz, cc):
        return wrap(zz, nz) * CORES + cc

    up_z, down_z, partner = dev(z + 1, c), dev(z - 1, c), dev(z, 1 - c)
    x_right, x_left = wrap(x + 1, tp), wrap(x - 1, tp)
    dl = 1 - 2 * c
    x_long, x_short = wrap(x + dl, tp), wrap(x - dl, tp)

    barrier = pltpu.get_barrier_semaphore()
    for who in ({"ep": up_z}, {"ep": down_z}, {"ep": partner}, {"tp": x_right}, {"tp": x_left}):
        pl.semaphore_signal(barrier, inc=1, device_id=who, device_id_type=MESH)

    def lanes(q):
        return pl.ds(pl.multiple_of(wrap(x - back + q, tp) * share, share), share)

    first = []
    for q in range(tp):
        first.append(pltpu.make_async_copy(tokens.at[:, lanes(q)], tok_in.at[q], in_sem.at[0, q]))
        first.append(pltpu.make_async_copy(norm_gain.at[:, lanes(q)], gain_in.at[q], in_sem.at[1, q]))
    first.append(pltpu.make_async_copy(routes, routes_in, in_sem.at[2, 0]))
    first.append(pltpu.make_async_copy(route_weights, weights_in, in_sem.at[2, 1]))
    first.append(pltpu.make_async_copy(final_gain, final_in, in_sem.at[2, 2]))
    for copy in first:
        copy.start()
    later = []
    for q in range(tp):
        later.append(pltpu.make_async_copy(w_gate.at[0, lanes(q), :], wgu.at[q, :, 0:share], in_sem.at[3, q]))
        later.append(pltpu.make_async_copy(w_up.at[0, lanes(q), :], wgu.at[q, :, share:2 * share], in_sem.at[4, q]))
        owner = pl.ds(pl.multiple_of(wrap(x + q * dl, tp) * share, share), share)
        later.append(pltpu.make_async_copy(w_down.at[0, :, owner], wd.at[q], in_sem.at[5, q]))
    for copy in later:
        copy.start()
    for copy in first:
        copy.wait()

    total = jnp.zeros((blk, 1), F32)
    for q in range(tp):
        value = tok_in[q].astype(F32)
        total = total + jnp.sum(value * value, axis=1, keepdims=True)
    inverse = lax.rsqrt(total / (tp * share) + EPS)
    for q in range(zs):
        value = tok_in[q].astype(F32) * inverse * gain_in[q]
        tok[last, q, blk:2 * blk, :] = value.astype(BF16)

    expert_ids = lax.broadcasted_iota(I32, (blk, ep), 1)
    hits = jnp.zeros((blk, ep), F32)
    wt = jnp.zeros((blk, ep), F32)
    for k in range(TOP_K):
        hit = routes_in[:, k:k + 1] == expert_ids
        hits = hits + jnp.where(hit, 1.0, 0.0)
        wt = wt + jnp.where(hit, weights_in[:, k:k + 1], 0.0)
    hits_b = hits.astype(BF16)
    row_t = lax.broadcasted_iota(I32, (blk, 2 * blk), 0)
    lane_t = lax.broadcasted_iota(I32, (blk, 2 * blk), 1)
    lane_t = jnp.where(lane_t >= blk, lane_t - blk, lane_t)
    earlier = jnp.where(row_t < lane_t, 1.0, 0.0).astype(BF16)
    same = jnp.where(row_t == lane_t, 1.0, 0.0).astype(BF16)
    over = (((0,), (0,)), ((), ()))
    slot_t = lax.dot_general(hits_b, earlier, over, preferred_element_type=F32)
    hits_t = lax.dot_general(hits_b, same, over, preferred_element_type=F32)
    tab[last, 1] = (hits_t * (slot_t + 1.0)).astype(BF16)

    own = slice(blk, 2 * blk)
    plus, minus = slice(0, blk), slice(blk, 2 * blk)
    halves = (slice(0, half), slice(half, zs))

    def z_copy(dst_slot, way, piece, to, src_slot, src_tok, src_tab, dst_tok, dst_tab):
        if piece < 2:
            src, dst = tok.at[src_slot, halves[piece], src_tok, :], tok.at[dst_slot, halves[piece], dst_tok, :]
        else:
            src, dst = tab.at[src_slot, src_tab], tab.at[dst_slot, dst_tab]
        return pltpu.make_async_remote_copy(
            src, dst, z_send.at[dst_slot, way, piece], z_recv.at[dst_slot, way, piece],
            device_id={"ep": to}, device_id_type=MESH)

    def z_own(way, piece):
        return z_copy(0, way, piece, (up_z, down_z)[way], last, own, 1, (plus, minus)[way], way)

    def z_next(slot, way, piece):
        where = (plus, minus)[way]
        return z_copy(slot + 1, way, piece, (up_z, down_z)[way], slot, where, way, where, way)

    def z_end(piece):
        there = pl.ds(pl.multiple_of(c * blk, blk), blk)
        return z_copy(last, 0, piece, jnp.where(c == 0, up_z, down_z), last - 1, there, c, plus, 0)

    def z_done(slot, way, piece):
        where = (plus, minus)[way]
        ref = tok.at[slot, halves[piece], where, :] if piece < 2 else tab.at[slot, way]
        return pltpu.make_async_remote_copy(
            ref, ref, z_send.at[slot, way, piece], z_recv.at[slot, way, piece],
            device_id={"ep": up_z}, device_id_type=MESH)

    pl.semaphore_wait(barrier, 5)
    for piece in (2, 0, 1):
        for way in range(2):
            z_own(way, piece).start()

    t_row = lax.broadcasted_iota(I32, (blk, blk), 0)
    t_col = lax.broadcasted_iota(I32, (blk, blk), 1)
    before = jnp.where(t_col < t_row, 1.0, 0.0).astype(BF16)
    slot = jnp.dot(before, hits_b, preferred_element_type=F32)
    slot1 = (hits * (slot + 1.0)).astype(BF16)
    lane = lax.broadcasted_iota(I32, (ep, ep * cap), 1)
    start = lax.broadcasted_iota(I32, (ep, ep * cap), 0) * cap
    past = lane >= start
    inside = jnp.where(past & (lane < start + cap), 1.0, 0.0)
    spread = inside.astype(BF16)
    want = jnp.sum(inside * (lane - start + 1).astype(F32), axis=0, keepdims=True)
    wt_hi = wt.astype(BF16)
    wt_lo = (wt - wt_hi.astype(F32)).astype(BF16)
    match = jnp.dot(slot1, spread, preferred_element_type=F32) == want
    c_hi[...] = jnp.where(match, jnp.dot(wt_hi, spread, preferred_element_type=F32), 0.0).astype(BF16)
    c_lo[...] = jnp.where(match, jnp.dot(wt_lo, spread, preferred_element_type=F32), 0.0).astype(BF16)

    for copy in later:
        copy.wait()

    def d_copy(slot, piece):
        if piece < 2:
            src, dst = tok.at[slot, halves[piece], 0:2 * blk, :], tok.at[slot, halves[piece], 2 * blk:4 * blk, :]
        else:
            src, dst = tab.at[slot, 0:2], tab.at[slot, 2:4]
        return pltpu.make_async_remote_copy(
            src, dst, d_send.at[slot, piece], d_recv.at[slot, piece],
            device_id={"ep": partner}, device_id_type=MESH)

    def x_copy(slot, way):
        src, dst, to = ((zs - 1, tp - 2, x_left), (0, tp - 1, x_right))[way]
        return pltpu.make_async_remote_copy(
            rows.at[slot, src], rows.at[slot, dst], x_send.at[slot, way], x_recv.at[slot, way],
            device_id={"tp": to}, device_id_type=MESH)

    def long_copy(slot, hop):
        src = part.at[slot, hl] if hop == 1 else rs_long.at[slot, hop - 2]
        return pltpu.make_async_remote_copy(
            src, rs_long.at[slot, hop - 1], l_send.at[slot, hop - 1], l_recv.at[slot, hop - 1],
            device_id={"tp": x_long}, device_id_type=MESH)

    def short_copy(slot, hop):
        src = part.at[slot, tp - hs] if hop == 1 else rs_short.at[slot, hop - 2]
        return pltpu.make_async_remote_copy(
            src, rs_short.at[slot, hop - 1], s_send.at[slot, hop - 1], s_recv.at[slot, hop - 1],
            device_id={"tp": x_short}, device_id_type=MESH)

    def ret_copy(slot, j, to):
        return pltpu.make_async_remote_copy(
            ret.at[slot, j], results.at[e], r_send.at[slot, j], r_recv.at[0],
            device_id={"ep": to}, device_id_type=MESH)

    def arrive(slot, piece):
        @pl.when(slot < last)
        def _():
            z_done(slot, 0, piece).wait_recv()
            z_done(slot, 1, piece).wait_recv()

            @pl.when(slot < last - 1)
            def _():
                z_next(slot, 0, piece).start()
                z_next(slot, 1, piece).start()

            @pl.when(slot == last - 1)
            def _():
                z_end(piece).start()

        @pl.when(slot == last)
        def _():
            z_done(slot, 0, piece).wait_recv()

        @pl.when(slot <= last)
        def _():
            d_copy(slot, piece).start()

    rows_all = 4 * cap
    r_id = lax.broadcasted_iota(I32, (rows_all, 4 * blk), 0)
    l_id = lax.broadcasted_iota(I32, (rows_all, 4 * blk), 1)
    my_slot = jnp.full((rows_all, 4 * blk), -1.0, F32)
    for j in range(4):
        good = (r_id >= j * cap) & (r_id < (j + 1) * cap) & (l_id >= j * blk) & (l_id < (j + 1) * blk)
        my_slot = jnp.where(good, (r_id - j * cap + 1).astype(F32), my_slot)
    left_half = lax.broadcasted_iota(I32, (1, 2 * blk), 1) < blk
    my_expert = lax.broadcasted_iota(I32, (ep, 2 * blk), 0) == e

    def pick(slot):
        for piece in range(3):
            d_copy(slot, piece).wait_recv()
        seen = []
        for j in range(4):
            seen.append(jnp.sum(jnp.where(my_expert, tab[slot, j].astype(F32), 0.0), axis=0, keepdims=True))
        pair = jnp.concatenate(
            [jnp.where(left_half, seen[0], seen[1]), jnp.where(left_half, seen[2], seen[3])], axis=1)
        choose = jnp.where(my_slot == pair, 1.0, 0.0).astype(BF16)

        def one(q):
            rows[slot, q] = jnp.dot(choose, tok[slot, q], preferred_element_type=F32).astype(BF16)

        one(zs - 1)
        x_copy(slot, 0).start()
        one(0)
        x_copy(slot, 1).start()
        for q in range(1, zs - 1):
            one(q)

    def compute(slot):
        acc = jnp.zeros((rows_all, 2 * share), F32)
        for q in range(zs):
            acc = acc + jnp.dot(rows[slot, q], wgu[q], preferred_element_type=F32)
        x_copy(slot, 0).wait_recv()
        x_copy(slot, 1).wait_recv()
        for q in range(zs, tp):
            acc = acc + jnp.dot(rows[slot, q], wgu[q], preferred_element_type=F32)
        gate, up = acc[:, :share], acc[:, share:]
        hidden = (gate / (1.0 + jnp.exp(-gate)) * up).astype(BF16)

        def one(q):
            part[slot, q] = jnp.dot(hidden, wd[q], preferred_element_type=F32).astype(BF16)

        one(hl)
        long_copy(slot, 1).start()
        one(tp - hs)
        short_copy(slot, 1).start()
        for q in range(tp):
            if q not in (hl, tp - hs):
                one(q)

    def hop(slot, h):
        long_copy(slot, h).wait_recv()
        rs_long[slot, h - 1] = (rs_long[slot, h - 1].astype(F32) + part[slot, hl - h].astype(F32)).astype(BF16)
        long_copy(slot, h + 1).start()
        if h < hs:
            short_copy(slot, h).wait_recv()
            rs_short[slot, h - 1] = (
                rs_short[slot, h - 1].astype(F32) + part[slot, tp - hs + h].astype(F32)).astype(BF16)
            short_copy(slot, h + 1).start()

    def finish(slot):
        long_copy(slot, hl).wait_recv()
        short_copy(slot, hs).wait_recv()
        value = part[slot, 0].astype(F32) + rs_long[slot, hl - 1].astype(F32) + rs_short[slot, hs - 1].astype(F32)
        for j in range(4):
            ret[slot, j] = value[j * cap:(j + 1) * cap].astype(BF16)

        @pl.when(slot < last)
        def _():
            for j in range(4):
                ret_copy(slot, j, dev(z + (-1, 1)[j % 2] * (slot + 1), (c, 1 - c)[j // 2])).start()

        @pl.when(slot == last)
        def _():
            ret_copy(slot, 0, dev(z + steps, c)).start()
            ret_copy(slot, 2, dev(z + steps, 1 - c)).start()
            ret_copy(slot, 3, partner).start()
            results[e] = ret[slot, 1]

    def at(turn, behind, act):
        @pl.when((turn >= behind) & (turn - behind <= last))
        def _():
            act(turn - behind)

    def turn(t, carry):
        arrive(t, 2)
        arrive(t, 0)
        at(t, hl + 1, finish)
        for h in range(hl - 1, 0, -1):
            at(t, h + 1, lambda s, h=h: hop(s, h))
        at(t, 1, compute)
        arrive(t, 1)
        at(t, 0, pick)
        return carry

    lax.fori_loop(0, steps + hl + 1, turn, 0)

    pltpu.make_async_copy(results.at[0:ep - 1], results.at[0:ep - 1], r_recv.at[0]).wait()
    got = results[...].astype(F32).reshape(ep * cap, share).astype(BF16)
    combined = jnp.dot(c_hi[...], got, preferred_element_type=F32) + jnp.dot(
        c_lo[...], got, preferred_element_type=F32)
    own_sq = jnp.sum(combined * combined, axis=1, keepdims=True)
    eye = t_row == t_col
    flat = jnp.sum(jnp.where(eye, jnp.broadcast_to(own_sq, (blk, blk)), 0.0), axis=0, keepdims=True)
    squares[x] = jnp.broadcast_to(jnp.concatenate([flat, flat], axis=1), squares.shape[1:])

    def q_copy(q):
        return pltpu.make_async_remote_copy(
            squares.at[x], squares.at[x], q_send.at[q], q_recv.at[0],
            device_id={"tp": wrap(x + q, tp)}, device_id_type=MESH)

    for q in range(1, tp):
        q_copy(q).start()

    def drain(slot, carry):
        for piece in range(3):
            d_copy(slot, piece).wait_send()

            @pl.when(slot < last)
            def _(piece=piece):
                z_done(slot, 0, piece).wait_send()
                z_done(slot, 1, piece).wait_send()

            @pl.when(slot == last)
            def _(piece=piece):
                z_done(slot, 0, piece).wait_send()
        for way in range(2):
            x_copy(slot, way).wait_send()
        for h in range(1, hl + 1):
            long_copy(slot, h).wait_send()
        for h in range(1, hs + 1):
            short_copy(slot, h).wait_send()
        for j in (0, 2, 3):
            ret_copy(slot, j, partner).wait_send()

        @pl.when(slot < last)
        def _():
            ret_copy(slot, 1, partner).wait_send()

        return carry

    lax.fori_loop(0, steps, drain, 0)
    for q in range(1, tp):
        q_copy(q).wait_send()
    pltpu.make_async_copy(squares.at[0:tp - 1], squares.at[0:tp - 1], q_recv.at[0]).wait()
    everyone = jnp.sum(squares[...], axis=0)[0:1, 0:blk]
    column = jnp.sum(jnp.where(eye, jnp.broadcast_to(everyone, (blk, blk)), 0.0), axis=1, keepdims=True)
    scale = lax.rsqrt(column / (tp * share) + EPS)
    out[...] = (combined * scale * final_in[...]).astype(out.dtype)


def solution(mesh):
    ep, tp = mesh.shape["ep"], mesh.shape["tp"]

    def per_device(tokens, norm_gain, routes, route_weights, w_gate, w_up, w_down, final_gain):
        blk, features = tokens.shape
        cap = max(2, min(blk, 2 * blk * TOP_K // ep))
        share = features // tp
        steps = ep // CORES // 2
        hl, hs = tp // 2, tp - 1 - tp // 2
        zs = tp - 2
        dma = pltpu.SemaphoreType.DMA
        vmem = pltpu.VMEM
        return pl.pallas_call(
            functools.partial(kernel, ep, tp, cap),
            out_shape=jax.ShapeDtypeStruct((blk, share), BF16),
            in_specs=[pl.BlockSpec(memory_space=pl.ANY)] * 8,
            out_specs=pl.BlockSpec(memory_space=pltpu.VMEM),
            scratch_shapes=[
                vmem((steps, zs, 4 * blk, share), BF16),
                vmem((steps, 4, ep, 2 * blk), BF16),
                vmem((steps, tp, 4 * cap, share), BF16),
                vmem((steps, tp, 4 * cap, share), BF16),
                vmem((steps, hl, 4 * cap, share), BF16),
                vmem((steps, hs, 4 * cap, share), BF16),
                vmem((steps, 4, cap, share), BF16),
                vmem((ep, cap, share), BF16),
                vmem((tp, 8, 2 * blk), F32),
                vmem((tp, blk, share), BF16),
                vmem((tp, 1, share), F32),
                vmem((blk, TOP_K), I32),
                vmem((blk, TOP_K), F32),
                vmem((tp, share, 2 * share), BF16),
                vmem((tp, share, share), BF16),
                vmem((1, share), F32),
                vmem((blk, ep * cap), BF16),
                vmem((blk, ep * cap), BF16),
                dma((6, tp)),
                dma((steps, 2, 3)), dma((steps, 2, 3)),
                dma((steps, 3)), dma((steps, 3)),
                dma((steps, 2)), dma((steps, 2)),
                dma((steps, hl)), dma((steps, hl)),
                dma((steps, hs)), dma((steps, hs)),
                dma((steps, 4)), dma((1,)),
                dma((tp,)), dma((1,)),
            ],
            compiler_params=pltpu.CompilerParams(
                collective_id=0, has_side_effects=True, vmem_limit_bytes=56 * 1024 * 1024),
        )(tokens, norm_gain.reshape(1, features), routes, route_weights, w_gate, w_up, w_down,
          final_gain.reshape(1, share))

    placed = (
        P(("grp", "ep"), None),
        P(),
        P(("grp", "ep"), None),
        P(("grp", "ep"), None),
        P("ep", None, "tp"),
        P("ep", None, "tp"),
        P("ep", "tp", None),
        P("tp"),
    )
    return jax.shard_map(
        per_device, mesh=mesh, in_specs=placed, out_specs=P(("grp", "ep"), "tp"), check_vma=False
    )
```

time: 289 us -> 128 us (0.44)
  blocking collectives: 200 us -> 0 us
  Pallas kernels: 0 us -> 124 us
  waiting for transfers between devices: 50.1 us -> 0 us
  between operations: 13.5 us -> 0.01 us
  matrix products: 11.6 us -> 0 us
  other arithmetic: 8.04 us -> 0 us
    all_to_all x4 -> x0, blocking collectives: 200 us -> none  [the longest x1 72.6 us: per_device(): lax.all_to_all(outgoing, 'ep', split_axis=0, concat_axis=0, tiled=True)]
    pallas_call x0 -> x1, Pallas kernels: none -> 124 us  [per_device(): pl.pallas_call(functools.partial(kernel, ep, tp, cap), out_shape=jax.Shap...]
    all_gather x1 -> x0, waiting for transfers between devices: 50 us -> none  [per_device(): lax.all_gather(lax.all_to_all(outgoing, 'ep', split_axis=0, concat_axis=0...]
    dot_general x4 -> x0, matrix products: 11.6 us -> none  [the longest x1 7.17 us: per_device(): jnp.einsum('secf,efd->secd', hidden, w_down, preferred_element_type=jnp.f...]
    reduce_sum x5 -> x0, other arithmetic: 4.7 us -> none  [the longest x1 2.49 us: sum_at_owner(): return arrived.astype(jnp.float32).sum(axis=0)]
  transfers between devices with their start and end apart: 1 -> 0, of which waited for: 1 -> 0; matrix products, arithmetic and copies ran while one was open for 0% -> 0% of each run, Pallas kernels for 0% -> 0%
where the time goes in v1:
time: 128 us
  Pallas kernels  124 us (97%)
  local copies, waits for them, and re-layouts  3.49 us (3%)
    pallas_call x1, Pallas kernels, per_device(): pl.pallas_call(functools.partial(kernel, ep, tp, cap), out_shape=jax.Shap...  124 us
    unnamed x5, local copies, waits for them, and re-layouts  3.49 us

profile of v1, /device:TPU:65, one launch (start us, length us, event | category | flops | bytes accessed | tf_op | source)
XLA Modules:
  0.0 127.8 jit_solution(15300379675942863416)
XLA Ops:
  0.0 0.0 copy-start
  0.0 1.4 %copy.9.routes = s32[64,6]{1,0:T(8,128)} copy(s32[64,6]{0,1:T(8,128)} %param.10) | data formatting | bytes 3072 | tf_op args[2]
  1.4 0.0 copy-done
  1.4 0.7 copy.10.route_weights
  2.1 124.3 %shard_map.82 = bf16[64,256]{1,0:T(8,128)(2,1)} custom-call(bf16[64,2048]{1,0:T(8,128)(2,1)} %tokens.1, f32[1,2048]{1,0:T(1,128)} %bitcast.2, s32[64,6]{1,0:T(8,128)} %copy.9.routes, f32[64,6]{1,0:T(8,128)} %copy.10.route_weights, bf16[1,2048,256]{2,1,0:T(8,128)(2,1)} %w_gate.1, bf16[1,2048,256]{2,1,0:T(8,128)(2,1)} %w_up.1, bf16[1,256,2048]{2,1,0:T(8,128)(2,1)} %w_down.1, ...), custom_call_target="tpu_custom_call" | custom-call | tf_op jit(solution)/shard_map/pallas_call | solution.py:381
  126.4 1.4 %copy.12 = bf16[64,256]{1,0:T(8,128)(2,1)} copy(bf16[64,256]{1,0:T(8,128)(2,1)} %shard_map.82) | data formatting | bytes 65536
Async XLA Ops:
  0.0 1.4 %copy-start = (f32[64,6]{0,1:T(8,128)S(1)}, f32[64,6]{0,1:T(8,128)}, u32[]{:S(2)}) copy-start(f32[64,6]{0,1:T(8,128)} %param.11) | copy-start | bytes 4612

commit v2 on v1

v2 whole, which is shorter than its diff:
```python
import functools

import jax
import jax.numpy as jnp
from jax import lax
from jax.experimental import pallas as pl
from jax.experimental.pallas import tpu as pltpu
from jax.sharding import PartitionSpec as P

TOP_K = 6
EPS = 1e-06
MESH = pl.DeviceIdType.MESH
BF16, F32, I32 = jnp.bfloat16, jnp.float32, jnp.int32
CORES = 2


def wrap(value, count):
    return lax.rem(value + 4 * count, count)


def kernel(
    ep, tp, cap,
    tokens, norm_gain, routes, route_weights, w_gate, w_up, w_down, final_gain,
    out,
    tok, tab, rows, part, rs_long, rs_short, ret, results, squares,
    tok_in, gain_in, routes_in, weights_in, wgu, wd, final_in, c_hi, c_lo,
    in_sem, z_send, z_recv, d_send, d_recv, x_send, x_recv, l_send, l_recv, s_send, s_recv,
    r_send, r_recv, q_send, q_recv,
):
    e = lax.axis_index("ep")
    x = lax.axis_index("tp")
    z, c = lax.div(e, CORES), lax.rem(e, CORES)
    nz = ep // CORES
    steps = nz // 2
    zs = tp - 2
    back = tp // 2 - 2
    hl, hs = tp // 2, tp - 1 - tp // 2
    blk = tok_in.shape[1]
    share = tok_in.shape[2]
    last, mine = steps - 1, steps
    half = zs // 2

    def dev(zz, cc):
        return wrap(zz, nz) * CORES + cc

    up_z, down_z, partner = dev(z + 1, c), dev(z - 1, c), dev(z, 1 - c)
    x_right, x_left = wrap(x + 1, tp), wrap(x - 1, tp)
    dl = 1 - 2 * c
    x_long, x_short = wrap(x + dl, tp), wrap(x - dl, tp)

    barrier = pltpu.get_barrier_semaphore()
    for who in ({"ep": up_z}, {"ep": down_z}, {"ep": partner}, {"tp": x_right}, {"tp": x_left}):
        pl.semaphore_signal(barrier, inc=1, device_id=who, device_id_type=MESH)

    def lanes(q):
        return pl.ds(pl.multiple_of(wrap(x - back + q, tp) * share, share), share)

    first, second, later = [], [], []
    for q in range(tp):
        first.append(pltpu.make_async_copy(tokens.at[:, lanes(q)], tok_in.at[q], in_sem.at[0, q]))
        first.append(pltpu.make_async_copy(norm_gain.at[:, lanes(q)], gain_in.at[q], in_sem.at[1, q]))
    second.append(pltpu.make_async_copy(routes, routes_in, in_sem.at[2, 0]))
    second.append(pltpu.make_async_copy(route_weights, weights_in, in_sem.at[2, 1]))
    second.append(pltpu.make_async_copy(final_gain, final_in, in_sem.at[2, 2]))
    for q in range(tp):
        rows_q = slice(q * share, (q + 1) * share)
        later.append(pltpu.make_async_copy(w_gate.at[0, lanes(q), :], wgu.at[rows_q, 0:share], in_sem.at[3, q]))
        later.append(pltpu.make_async_copy(w_up.at[0, lanes(q), :], wgu.at[rows_q, share:2 * share], in_sem.at[4, q]))
        owner = pl.ds(pl.multiple_of(wrap(x + q * dl, tp) * share, share), share)
        later.append(pltpu.make_async_copy(w_down.at[0, :, owner], wd.at[q], in_sem.at[5, q]))
    for copy in first + second + later:
        copy.start()

    near, far = slice(0, blk), slice(blk, 2 * blk)
    halves = (slice(0, half), slice(half, zs))

    def z_copy(dst_slot, way, piece, to, src_slot, src_tok, src_tab, dst_tok, dst_tab):
        if piece < 2:
            src, dst = tok.at[src_slot, halves[piece], src_tok, :], tok.at[dst_slot, halves[piece], dst_tok, :]
        else:
            src, dst = tab.at[src_slot, src_tab], tab.at[dst_slot, dst_tab]
        return pltpu.make_async_remote_copy(
            src, dst, z_send.at[dst_slot, way, piece], z_recv.at[dst_slot, way, piece],
            device_id={"ep": to}, device_id_type=MESH)

    def z_own(way, piece):
        return z_copy(0, way, piece, (up_z, down_z)[way], mine, near, 0, (near, far)[way], way)

    def z_next(slot, way, piece):
        where = (near, far)[way]
        return z_copy(slot + 1, way, piece, (up_z, down_z)[way], slot, where, way, where, way)

    def z_end(piece):
        there = pl.ds(pl.multiple_of(c * blk, blk), blk)
        return z_copy(last, 0, piece, jnp.where(c == 0, up_z, down_z), last - 1, there, c, near, 0)

    def z_done(slot, way, piece):
        where = (near, far)[way]
        ref = tok.at[slot, halves[piece], where, :] if piece < 2 else tab.at[slot, way]
        return pltpu.make_async_remote_copy(
            ref, ref, z_send.at[slot, way, piece], z_recv.at[slot, way, piece],
            device_id={"ep": up_z}, device_id_type=MESH)

    def d_copy(slot, piece, n):
        h = n // 2
        if piece < 2:
            src = tok.at[slot, halves[piece], 0:h * blk, :]
            dst = tok.at[slot, halves[piece], h * blk:n * blk, :]
        else:
            src, dst = tab.at[slot, 0:h], tab.at[slot, h:n]
        return pltpu.make_async_remote_copy(
            src, dst, d_send.at[slot, piece], d_recv.at[slot, piece],
            device_id={"ep": partner}, device_id_type=MESH)

    def x_copy(slot, way, n):
        src, dst, to = ((zs - 1, tp - 2, x_left), (0, tp - 1, x_right))[way]
        return pltpu.make_async_remote_copy(
            rows.at[slot, 0:n * cap, src * share:(src + 1) * share],
            rows.at[slot, 0:n * cap, dst * share:(dst + 1) * share],
            x_send.at[slot, way], x_recv.at[slot, way], device_id={"tp": to}, device_id_type=MESH)

    def long_copy(slot, hop, n):
        top = slice(0, n * cap)
        src = part.at[slot, hl, top] if hop == 1 else rs_long.at[slot, hop - 2, top]
        return pltpu.make_async_remote_copy(
            src, rs_long.at[slot, hop - 1, top], l_send.at[slot, hop - 1], l_recv.at[slot, hop - 1],
            device_id={"tp": x_long}, device_id_type=MESH)

    def short_copy(slot, hop, n):
        top = slice(0, n * cap)
        src = part.at[slot, tp - hs, top] if hop == 1 else rs_short.at[slot, hop - 2, top]
        return pltpu.make_async_remote_copy(
            src, rs_short.at[slot, hop - 1, top], s_send.at[slot, hop - 1], s_recv.at[slot, hop - 1],
            device_id={"tp": x_short}, device_id_type=MESH)

    def ret_copy(slot, j, to):
        return pltpu.make_async_remote_copy(
            ret.at[slot, j], results.at[e], r_send.at[slot, j], r_recv.at[0],
            device_id={"ep": to}, device_id_type=MESH)

    for copy in first:
        copy.wait()
    total = jnp.zeros((blk, 1), F32)
    for q in range(tp):
        value = tok_in[q].astype(F32)
        total = total + jnp.sum(value * value, axis=1, keepdims=True)
    inverse = lax.rsqrt(total / (tp * share) + EPS)

    def norm(q):
        value = tok_in[q].astype(F32) * inverse * gain_in[q]
        tok[mine, q, near, :] = value.astype(BF16)

    for q in range(half):
        norm(q)
    pl.semaphore_wait(barrier, 5)
    z_own(0, 0).start()
    z_own(1, 0).start()
    for q in range(half, zs):
        norm(q)
    z_own(0, 1).start()
    z_own(1, 1).start()
    d_copy(mine, 0, 2).start()
    d_copy(mine, 1, 2).start()

    for copy in second:
        copy.wait()
    expert_ids = lax.broadcasted_iota(I32, (ep, blk), 0)
    hits = jnp.zeros((ep, blk), F32)
    wt = jnp.zeros((ep, blk), F32)
    for k in range(TOP_K):
        hit = routes_in[k:k + 1, :] == expert_ids
        hits = hits + jnp.where(hit, 1.0, 0.0)
        wt = wt + jnp.where(hit, weights_in[k:k + 1, :], 0.0)
    hits_b = hits.astype(BF16)
    row_t = lax.broadcasted_iota(I32, (blk, 2 * blk), 0)
    lane_t = lax.broadcasted_iota(I32, (blk, 2 * blk), 1)
    lane_t = jnp.where(lane_t >= blk, lane_t - blk, lane_t)
    earlier = jnp.where(row_t < lane_t, 1.0, 0.0).astype(BF16)
    same = jnp.where(row_t == lane_t, 1.0, 0.0).astype(BF16)
    slots = jnp.dot(hits_b, same, preferred_element_type=F32) * (
        jnp.dot(hits_b, earlier, preferred_element_type=F32) + 1.0)
    tab[mine, 0] = slots.astype(BF16)
    z_own(0, 2).start()
    z_own(1, 2).start()
    d_copy(mine, 2, 2).start()

    over = (((0,), (0,)), ((), ()))
    slot1 = slots[:, 0:blk].astype(BF16)
    lane = lax.broadcasted_iota(I32, (ep, ep * cap), 1)
    start = lax.broadcasted_iota(I32, (ep, ep * cap), 0) * cap
    inside = jnp.where((lane >= start) & (lane < start + cap), 1.0, 0.0)
    spread = inside.astype(BF16)
    want = jnp.sum(inside * (lane - start + 1).astype(F32), axis=0, keepdims=True)
    wt_hi = wt.astype(BF16)
    wt_lo = (wt - wt_hi.astype(F32)).astype(BF16)
    match = lax.dot_general(slot1, spread, over, preferred_element_type=F32) == want
    c_hi[...] = jnp.where(
        match, lax.dot_general(wt_hi, spread, over, preferred_element_type=F32), 0.0).astype(BF16)
    c_lo[...] = jnp.where(
        match, lax.dot_general(wt_lo, spread, over, preferred_element_type=F32), 0.0).astype(BF16)

    for copy in later:
        copy.wait()

    def arrive(slot, piece):
        @pl.when(slot < last)
        def _():
            z_done(slot, 0, piece).wait_recv()
            z_done(slot, 1, piece).wait_recv()

            @pl.when(slot < last - 1)
            def _():
                z_next(slot, 0, piece).start()
                z_next(slot, 1, piece).start()

            @pl.when(slot == last - 1)
            def _():
                z_end(piece).start()

            d_copy(slot, piece, 4).start()

        @pl.when(slot == last)
        def _():
            z_done(slot, 0, piece).wait_recv()
            d_copy(slot, piece, 2).start()

    left_half = lax.broadcasted_iota(I32, (1, 2 * blk), 1) < blk
    my_expert = lax.broadcasted_iota(I32, (ep, 2 * blk), 0) == e

    def pick(slot, n):
        r_id = lax.broadcasted_iota(I32, (n * cap, n * blk), 0)
        l_id = lax.broadcasted_iota(I32, (n * cap, n * blk), 1)
        my_slot = jnp.full((n * cap, n * blk), -1, I32)
        for j in range(n):
            good = (r_id >= j * cap) & (r_id < (j + 1) * cap) & (l_id >= j * blk) & (l_id < (j + 1) * blk)
            my_slot = jnp.where(good, r_id - j * cap + 1, my_slot)
        for piece in range(3):
            d_copy(slot, piece, n).wait_recv()
        seen = []
        for j in range(n):
            seen.append(jnp.sum(jnp.where(my_expert, tab[slot, j].astype(F32), 0.0), axis=0, keepdims=True))
        pair = jnp.concatenate(
            [jnp.where(left_half, seen[j], seen[j + 1]) for j in range(0, n, 2)], axis=1)
        choose = jnp.where(my_slot.astype(F32) == pair, 1.0, 0.0).astype(BF16)

        def one(q):
            rows[slot, 0:n * cap, q * share:(q + 1) * share] = jnp.dot(
                choose, tok[slot, q, 0:n * blk, :], preferred_element_type=F32).astype(BF16)

        one(zs - 1)
        x_copy(slot, 0, n).start()
        one(0)
        x_copy(slot, 1, n).start()
        for q in range(1, zs - 1):
            one(q)

    def compute(slot, n):
        x_copy(slot, 0, n).wait_recv()
        x_copy(slot, 1, n).wait_recv()
        acc = jnp.dot(rows[slot, 0:n * cap, :], wgu[...], preferred_element_type=F32)
        gate, up = acc[:, :share], acc[:, share:]
        hidden = (gate / (1.0 + jnp.exp(-gate)) * up).astype(BF16)

        def one(q):
            part[slot, q, 0:n * cap] = jnp.dot(hidden, wd[q], preferred_element_type=F32).astype(BF16)

        one(hl)
        long_copy(slot, 1, n).start()
        one(tp - hs)
        short_copy(slot, 1, n).start()
        for q in range(tp):
            if q not in (hl, tp - hs):
                one(q)

    def hop(slot, n, h):
        top = slice(0, n * cap)
        long_copy(slot, h, n).wait_recv()
        rs_long[slot, h - 1, top] = (
            rs_long[slot, h - 1, top].astype(F32) + part[slot, hl - h, top].astype(F32)).astype(BF16)
        long_copy(slot, h + 1, n).start()
        if h < hs:
            short_copy(slot, h, n).wait_recv()
            rs_short[slot, h - 1, top] = (
                rs_short[slot, h - 1, top].astype(F32) + part[slot, tp - hs + h, top].astype(F32)).astype(BF16)
            short_copy(slot, h + 1, n).start()

    def finish(slot, n):
        top = slice(0, n * cap)
        long_copy(slot, hl, n).wait_recv()
        short_copy(slot, hs, n).wait_recv()
        value = (part[slot, 0, top].astype(F32) + rs_long[slot, hl - 1, top].astype(F32)
                 + rs_short[slot, hs - 1, top].astype(F32))
        for j in range(n):
            ret[slot, j] = value[j * cap:(j + 1) * cap].astype(BF16)
        if n == 4:
            for j in range(4):
                ret_copy(slot, j, dev(z + (-1, 1)[j % 2] * (slot + 1), (c, 1 - c)[j // 2])).start()
        else:
            @pl.when(slot == last)
            def _():
                ret_copy(slot, 0, dev(z + steps, c)).start()
                ret_copy(slot, 1, dev(z + steps, 1 - c)).start()

            @pl.when(slot == mine)
            def _():
                ret_copy(slot, 1, partner).start()
                results[e] = ret[slot, 0]

    def at(turn, behind, act):
        slot = turn - behind

        @pl.when((slot >= 0) & (slot < last))
        def _():
            act(slot, 4)

        @pl.when((slot == -1) | (slot == last))
        def _():
            act(jnp.where(slot < 0, mine, slot), 2)

    def turn(t, carry):
        arrive(t, 0)
        at(t, hl + 2, finish)
        for h in range(hl - 1, 0, -1):
            at(t, h + 2, functools.partial(hop, h=h))
        at(t, 1, pick)
        arrive(t, 1)
        arrive(t, 2)
        at(t, 2, compute)
        return carry

    lax.fori_loop(0, steps + hl + 2, turn, 0)

    pltpu.make_async_copy(results.at[0:ep - 1], results.at[0:ep - 1], r_recv.at[0]).wait()
    got = results[...].astype(F32).reshape(ep * cap, share).astype(BF16)
    combined = jnp.dot(c_hi[...], got, preferred_element_type=F32) + jnp.dot(
        c_lo[...], got, preferred_element_type=F32)
    own_sq = jnp.sum(combined * combined, axis=1, keepdims=True)
    eye = lax.broadcasted_iota(I32, (blk, blk), 0) == lax.broadcasted_iota(I32, (blk, blk), 1)
    flat = jnp.sum(jnp.where(eye, jnp.broadcast_to(own_sq, (blk, blk)), 0.0), axis=0, keepdims=True)
    squares[x] = jnp.broadcast_to(jnp.concatenate([flat, flat], axis=1), squares.shape[1:])

    def q_copy(q):
        return pltpu.make_async_remote_copy(
            squares.at[x], squares.at[x], q_send.at[q], q_recv.at[0],
            device_id={"tp": wrap(x + q, tp)}, device_id_type=MESH)

    for q in range(1, tp):
        q_copy(q).start()

    def left(slot, n):
        for piece in range(3):
            d_copy(slot, piece, n).wait_send()
        for way in range(2):
            x_copy(slot, way, n).wait_send()
        for h in range(1, hl + 1):
            long_copy(slot, h, n).wait_send()
        for h in range(1, hs + 1):
            short_copy(slot, h, n).wait_send()
        for j in range(1, n):
            ret_copy(slot, j, partner).wait_send()

    def drain(slot, carry):
        left(slot, 4)
        ret_copy(slot, 0, partner).wait_send()
        for piece in range(3):
            z_done(slot, 0, piece).wait_send()
            z_done(slot, 1, piece).wait_send()
        return carry

    lax.fori_loop(0, last, drain, 0)
    left(last, 2)
    left(mine, 2)
    ret_copy(last, 0, partner).wait_send()
    for piece in range(3):
        z_done(last, 0, piece).wait_send()
    for q in range(1, tp):
        q_copy(q).wait_send()
    pltpu.make_async_copy(squares.at[0:tp - 1], squares.at[0:tp - 1], q_recv.at[0]).wait()
    everyone = jnp.sum(squares[...], axis=0)[0:1, 0:blk]
    column = jnp.sum(jnp.where(eye, jnp.broadcast_to(everyone, (blk, blk)), 0.0), axis=1, keepdims=True)
    scale = lax.rsqrt(column / (tp * share) + EPS)
    out[...] = (combined * scale * final_in[...]).astype(out.dtype)


def solution(mesh):
    ep, tp = mesh.shape["ep"], mesh.shape["tp"]

    def per_device(tokens, norm_gain, routes, route_weights, w_gate, w_up, w_down, final_gain):
        blk, features = tokens.shape
        cap = max(2, min(blk, 2 * blk * TOP_K // ep))
        share = features // tp
        slots = ep // CORES // 2 + 1
        hl, hs = tp // 2, tp - 1 - tp // 2
        zs = tp - 2
        dma = pltpu.SemaphoreType.DMA
        vmem = pltpu.VMEM
        return pl.pallas_call(
            functools.partial(kernel, ep, tp, cap),
            out_shape=jax.ShapeDtypeStruct((blk, share), BF16),
            in_specs=[pl.BlockSpec(memory_space=pl.ANY)] * 8,
            out_specs=pl.BlockSpec(memory_space=pltpu.VMEM),
            scratch_shapes=[
                vmem((slots, zs, 4 * blk, share), BF16),
                vmem((slots, 4, ep, 2 * blk), BF16),
                vmem((slots, 4 * cap, features), BF16),
                vmem((slots, tp, 4 * cap, share), BF16),
                vmem((slots, hl, 4 * cap, share), BF16),
                vmem((slots, hs, 4 * cap, share), BF16),
                vmem((slots, 4, cap, share), BF16),
                vmem((ep, cap, share), BF16),
                vmem((tp, 8, 2 * blk), F32),
                vmem((tp, blk, share), BF16),
                vmem((tp, 1, share), F32),
                vmem((TOP_K, blk), I32),
                vmem((TOP_K, blk), F32),
                vmem((features, 2 * share), BF16),
                vmem((tp, share, share), BF16),
                vmem((1, share), F32),
                vmem((blk, ep * cap), BF16),
                vmem((blk, ep * cap), BF16),
                dma((6, tp)),
                dma((slots, 2, 3)), dma((slots, 2, 3)),
                dma((slots, 3)), dma((slots, 3)),
                dma((slots, 2)), dma((slots, 2)),
                dma((slots, hl)), dma((slots, hl)),
                dma((slots, hs)), dma((slots, hs)),
                dma((slots, 4)), dma((1,)),
                dma((tp,)), dma((1,)),
            ],
            compiler_params=pltpu.CompilerParams(
                collective_id=0, has_side_effects=True, vmem_limit_bytes=56 * 1024 * 1024),
        )(tokens, norm_gain.reshape(1, features), routes.T, route_weights.T, w_gate, w_up, w_down,
          final_gain.reshape(1, share))

    placed = (
        P(("grp", "ep"), None),
        P(),
        P(("grp", "ep"), None),
        P(("grp", "ep"), None),
        P("ep", None, "tp"),
        P("ep", None, "tp"),
        P("ep", "tp", None),
        P("tp"),
    )
    return jax.shard_map(
        per_device, mesh=mesh, in_specs=placed, out_specs=P(("grp", "ep"), "tp"), check_vma=False
    )
```

time: 128 us -> 125 us (0.977)
  local copies, waits for them, and re-layouts: 3.49 us -> 1.38 us
    unnamed x5 -> x1, local copies, waits for them, and re-layouts: 3.49 us -> 1.38 us
where the time goes in v2:
time: 125 us; the launch traced here: 124 us
  Pallas kernels  123 us (98%)
  local copies, waits for them, and re-layouts  1.38 us (1%)
    pallas_call x1, Pallas kernels, per_device(): pl.pallas_call(functools.partial(kernel, ep, tp, cap), out_shape=jax.Shap...  123 us

profile of v2, /device:TPU:65, one launch (start us, length us, event | category | flops | bytes accessed | tf_op | source)
XLA Modules:
  0.0 124.4 jit_solution(12252150090609049249)
XLA Ops:
  0.0 123.0 %shard_map.82 = bf16[64,256]{1,0:T(8,128)(2,1)} custom-call(bf16[64,2048]{1,0:T(8,128)(2,1)} %tokens.1, f32[1,2048]{1,0:T(1,128)} %bitcast.4, s32[6,64]{1,0:T(8,128)} %bitcast.5, f32[6,64]{1,0:T(8,128)} %bitcast.6, bf16[1,2048,256]{2,1,0:T(8,128)(2,1)} %w_gate.1, bf16[1,2048,256]{2,1,0:T(8,128)(2,1)} %w_up.1, bf16[1,256,2048]{2,1,0:T(8,128)(2,1)} %w_down.1, ...), custom_call_target="tpu_custom_call" | custom-call | tf_op jit(solution)/shard_map/pallas_call | solution.py:397
  123.1 1.4 %copy.10 = bf16[64,256]{1,0:T(8,128)(2,1)} copy(bf16[64,256]{1,0:T(8,128)(2,1)} %shard_map.82) | data formatting | bytes 65536

commit v3 on v2

v3 whole, which is shorter than its diff:
```python
import functools

import jax
import jax.numpy as jnp
from jax import lax
from jax.experimental import pallas as pl
from jax.experimental.pallas import tpu as pltpu
from jax.sharding import PartitionSpec as P

TOP_K = 6
EPS = 1e-06
MESH = pl.DeviceIdType.MESH
BF16, F32, I32 = jnp.bfloat16, jnp.float32, jnp.int32
CORES = 2
XS = 2


def wrap(value, count):
    return lax.rem(value + 4 * count, count)


def kernel(
    ep, tp, cap,
    tokens, norm_gain, routes, route_weights, w_gate, w_up, w_down, final_gain,
    out,
    tok, tab, rows, part, rs, direct, ret, results, squares,
    tok_in, gain_in, routes_in, weights_in, wgu, wd, final_in, c_hi, c_lo,
    in_sem, out_sem, z_recv, d_recv, x_recv, l_recv, t_recv, r_recv, q_recv,
):
    e = lax.axis_index("ep")
    x = lax.axis_index("tp")
    z, c = lax.div(e, CORES), lax.rem(e, CORES)
    nz = ep // CORES
    steps = nz // 2
    zs = tp - XS
    back = (zs - 1) // 2
    hl, hs = tp // 2, tp - 1 - tp // 2
    blk = tok_in.shape[1]
    share = tok_in.shape[2]
    last, mine = steps - 1, steps
    half = zs // 2

    def dev(zz, cc):
        return wrap(zz, nz) * CORES + cc

    up_z, down_z, partner = dev(z + 1, c), dev(z - 1, c), dev(z, 1 - c)
    x_right, x_left = wrap(x + 1, tp), wrap(x - 1, tp)
    dl = 1 - 2 * c
    x_long, x_short = wrap(x + dl, tp), wrap(x - dl, tp)

    barrier = pltpu.get_barrier_semaphore()
    for who in ({"ep": up_z}, {"ep": down_z}, {"ep": partner}, {"tp": x_right}, {"tp": x_left}):
        pl.semaphore_signal(barrier, inc=1, device_id=who, device_id_type=MESH)

    def lanes(q):
        return pl.ds(pl.multiple_of(wrap(x - back + q, tp) * share, share), share)

    for q in range(tp):
        pltpu.make_async_copy(tokens.at[:, lanes(q)], tok_in.at[q], in_sem.at[0]).start()
        pltpu.make_async_copy(norm_gain.at[:, lanes(q)], gain_in.at[q], in_sem.at[1]).start()
    second = [pltpu.make_async_copy(routes, routes_in, in_sem.at[2]),
              pltpu.make_async_copy(route_weights, weights_in, in_sem.at[3]),
              pltpu.make_async_copy(final_gain, final_in, in_sem.at[4])]
    for copy in second:
        copy.start()
    for q in range(tp):
        rows_q = slice(q * share, (q + 1) * share)
        pltpu.make_async_copy(w_gate.at[0, lanes(q), :], wgu.at[rows_q, 0:share], in_sem.at[5]).start()
        pltpu.make_async_copy(w_up.at[0, lanes(q), :], wgu.at[rows_q, share:2 * share], in_sem.at[5]).start()
        owner = pl.ds(pl.multiple_of(wrap(x + q * dl, tp) * share, share), share)
        pltpu.make_async_copy(w_down.at[0, :, owner], wd.at[q], in_sem.at[6]).start()

    def whole(ref, sem):
        return pltpu.make_async_copy(ref, ref, sem)

    near, far = slice(0, blk), slice(blk, 2 * blk)
    halves = (slice(0, half), slice(half, zs))

    def z_copy(dst_slot, piece, to, src_slot, src_tok, src_tab, dst_tok, dst_tab):
        if piece < 2:
            src, dst = tok.at[src_slot, halves[piece], src_tok, :], tok.at[dst_slot, halves[piece], dst_tok, :]
        else:
            src, dst = tab.at[src_slot, src_tab], tab.at[dst_slot, dst_tab]
        return pltpu.make_async_remote_copy(
            src, dst, out_sem.at[piece // 2], z_recv.at[dst_slot, piece],
            device_id={"ep": to}, device_id_type=MESH)

    def z_own(way, piece):
        return z_copy(0, piece, (up_z, down_z)[way], mine, near, 0, (near, far)[way], way)

    def z_next(slot, way, piece):
        where = (near, far)[way]
        return z_copy(slot + 1, piece, (up_z, down_z)[way], slot, where, way, where, way)

    def z_end(piece):
        there = pl.ds(pl.multiple_of(c * blk, blk), blk)
        return z_copy(last, piece, jnp.where(c == 0, up_z, down_z), last - 1, there, c, near, 0)

    def z_done(slot, piece, n):
        ref = tok.at[slot, halves[piece], 0:n * blk, :] if piece < 2 else tab.at[slot, 0:n]
        return whole(ref, z_recv.at[slot, piece])

    def d_copy(slot, piece, n):
        h = n // 2
        if piece < 2:
            src = tok.at[slot, halves[piece], 0:h * blk, :]
            dst = tok.at[slot, halves[piece], h * blk:n * blk, :]
        else:
            src, dst = tab.at[slot, 0:h], tab.at[slot, h:n]
        return pltpu.make_async_remote_copy(
            src, dst, out_sem.at[2 + piece // 2], d_recv.at[slot, piece // 2],
            device_id={"ep": partner}, device_id_type=MESH)

    def d_done(slot, n):
        whole(tok.at[slot, :, n // 2 * blk:n * blk, :], d_recv.at[slot, 0]).wait()
        whole(tab.at[slot, n // 2:n], d_recv.at[slot, 1]).wait()

    def x_copies(slot, n):
        def one(src, dst, to):
            return pltpu.make_async_remote_copy(
                rows.at[slot, 0:n * cap, src], rows.at[slot, 0:n * cap, dst * share:(dst + 1) * share],
                out_sem.at[4], x_recv.at[slot], device_id={"tp": to}, device_id_type=MESH)

        if XS == 2:
            return [one(slice((zs - 1) * share, zs * share), tp - 2, x_left), one(slice(0, share), tp - 1, x_right)]
        if XS == 1:
            return [one(pl.ds(pl.multiple_of((1 - c) * (zs - 1) * share, share), share), tp - 1, x_short)]
        return []

    def rs_copy(slot, n, hop, side):
        top = slice(0, n * cap)
        src = part.at[slot, (hl, tp - hs)[side], top] if hop == 1 else rs.at[slot, hop - 2, side, top]
        return pltpu.make_async_remote_copy(
            src, rs.at[slot, hop - 1, side, top], out_sem.at[5], l_recv.at[slot, hop - 1],
            device_id={"tp": (x_long, x_short)[side]}, device_id_type=MESH)

    def direct_copy(q):
        return pltpu.make_async_remote_copy(
            part.at[last, q, 0:2 * cap], direct.at[tp - q - 1], out_sem.at[6], t_recv.at[0],
            device_id={"tp": wrap(x + q * dl, tp)}, device_id_type=MESH)

    def ret_copy(slot, j, to):
        return pltpu.make_async_remote_copy(
            ret.at[slot, j], results.at[e], out_sem.at[7], r_recv.at[0],
            device_id={"ep": to}, device_id_type=MESH)

    whole(tok_in, in_sem.at[0]).wait()
    whole(gain_in, in_sem.at[1]).wait()
    total = jnp.zeros((blk, 1), F32)
    for q in range(tp):
        value = tok_in[q].astype(F32)
        total = total + jnp.sum(value * value, axis=1, keepdims=True)
    inverse = lax.rsqrt(total / (tp * share) + EPS)

    def norm(q):
        value = tok_in[q].astype(F32) * inverse * gain_in[q]
        tok[mine, q, near, :] = value.astype(BF16)

    for q in range(half):
        norm(q)
    pl.semaphore_wait(barrier, 5)
    z_own(0, 0).start()
    z_own(1, 0).start()
    for q in range(half, zs):
        norm(q)
    z_own(0, 1).start()
    z_own(1, 1).start()
    d_copy(mine, 0, 2).start()
    d_copy(mine, 1, 2).start()

    for copy in second:
        copy.wait()
    expert_ids = lax.broadcasted_iota(I32, (ep, blk), 0)
    hits = jnp.zeros((ep, blk), F32)
    wt = jnp.zeros((ep, blk), F32)
    for k in range(TOP_K):
        hit = routes_in[k:k + 1, :] == expert_ids
        hits = hits + jnp.where(hit, 1.0, 0.0)
        wt = wt + jnp.where(hit, weights_in[k:k + 1, :], 0.0)
    hits_b = hits.astype(BF16)
    row_t = lax.broadcasted_iota(I32, (blk, 2 * blk), 0)
    lane_t = lax.broadcasted_iota(I32, (blk, 2 * blk), 1)
    lane_t = jnp.where(lane_t >= blk, lane_t - blk, lane_t)
    earlier = jnp.where(row_t < lane_t, 1.0, 0.0).astype(BF16)
    same = jnp.where(row_t == lane_t, 1.0, 0.0).astype(BF16)
    slots = jnp.dot(hits_b, same, preferred_element_type=F32) * (
        jnp.dot(hits_b, earlier, preferred_element_type=F32) + 1.0)
    tab[mine, 0] = slots.astype(BF16)
    z_own(0, 2).start()
    z_own(1, 2).start()
    d_copy(mine, 2, 2).start()

    over = (((0,), (0,)), ((), ()))
    slot1 = slots[:, 0:blk].astype(BF16)
    lane = lax.broadcasted_iota(I32, (ep, ep * cap), 1)
    start = lax.broadcasted_iota(I32, (ep, ep * cap), 0) * cap
    inside = jnp.where((lane >= start) & (lane < start + cap), 1.0, 0.0)
    spread = inside.astype(BF16)
    want = jnp.sum(inside * (lane - start + 1).astype(F32), axis=0, keepdims=True)
    wt_hi = wt.astype(BF16)
    wt_lo = (wt - wt_hi.astype(F32)).astype(BF16)
    match = lax.dot_general(slot1, spread, over, preferred_element_type=F32) == want
    c_hi[...] = jnp.where(
        match, lax.dot_general(wt_hi, spread, over, preferred_element_type=F32), 0.0).astype(BF16)
    c_lo[...] = jnp.where(
        match, lax.dot_general(wt_lo, spread, over, preferred_element_type=F32), 0.0).astype(BF16)

    whole(wgu, in_sem.at[5]).wait()
    whole(wd, in_sem.at[6]).wait()

    def arrive(slot, piece):
        @pl.when(slot < last)
        def _():
            z_done(slot, piece, 2).wait()

            @pl.when(slot < last - 1)
            def _():
                z_next(slot, 0, piece).start()
                z_next(slot, 1, piece).start()

            @pl.when(slot == last - 1)
            def _():
                z_end(piece).start()

            d_copy(slot, piece, 4).start()

        @pl.when(slot == last)
        def _():
            z_done(slot, piece, 1).wait()
            d_copy(slot, piece, 2).start()

    left_half = lax.broadcasted_iota(I32, (1, 2 * blk), 1) < blk
    my_expert = lax.broadcasted_iota(I32, (ep, 2 * blk), 0) == e

    def pick(slot, n):
        r_id = lax.broadcasted_iota(I32, (n * cap, n * blk), 0)
        l_id = lax.broadcasted_iota(I32, (n * cap, n * blk), 1)
        my_slot = jnp.full((n * cap, n * blk), -1, I32)
        for j in range(n):
            good = (r_id >= j * cap) & (r_id < (j + 1) * cap) & (l_id >= j * blk) & (l_id < (j + 1) * blk)
            my_slot = jnp.where(good, r_id - j * cap + 1, my_slot)
        d_done(slot, n)
        seen = []
        for j in range(n):
            seen.append(jnp.sum(jnp.where(my_expert, tab[slot, j].astype(F32), 0.0), axis=0, keepdims=True))
        pair = jnp.concatenate(
            [jnp.where(left_half, seen[j], seen[j + 1]) for j in range(0, n, 2)], axis=1)
        choose = jnp.where(my_slot.astype(F32) == pair, 1.0, 0.0).astype(BF16)

        def one(q):
            rows[slot, 0:n * cap, q * share:(q + 1) * share] = jnp.dot(
                choose, tok[slot, q, 0:n * blk, :], preferred_element_type=F32).astype(BF16)

        early = (0, zs - 1) if XS else ()
        for q in early:
            one(q)
        for copy in x_copies(slot, n):
            copy.start()
        for q in range(zs):
            if q not in early:
                one(q)

    def compute(slot, n, ring=True):
        if XS:
            whole(rows.at[slot, 0:n * cap, zs * share:], x_recv.at[slot]).wait()
        acc = jnp.dot(rows[slot, 0:n * cap, :], wgu[...], preferred_element_type=F32)
        gate, up = acc[:, :share], acc[:, share:]
        hidden = (gate / (1.0 + jnp.exp(-gate)) * up).astype(BF16)
        order = sorted(range(tp), key=lambda q: -min(q, tp - q))
        if ring:
            order = [hl, tp - hs] + [q for q in order if q not in (hl, tp - hs)]
        for place, q in enumerate(order):
            part[slot, q, 0:n * cap] = jnp.dot(hidden, wd[q], preferred_element_type=F32).astype(BF16)
            if ring and place < 2:
                rs_copy(slot, n, 1, place).start()
            if not ring and q:
                direct_copy(q).start()

    def hop(slot, n, h):
        top = slice(0, n * cap)
        both = h <= hs
        whole(rs.at[slot, h - 1, :, top] if both else rs.at[slot, h - 1, 0, top], l_recv.at[slot, h - 1]).wait()

        def add(side, q):
            rs[slot, h - 1, side, top] = (
                rs[slot, h - 1, side, top].astype(F32) + part[slot, q, top].astype(F32)).astype(BF16)
            rs_copy(slot, n, h + 1, side).start()

        add(0, hl - h)
        if h < hs:
            add(1, tp - hs + h)

    def give(slot, n, value):
        for j in range(n):
            ret[slot, j] = value[j * cap:(j + 1) * cap].astype(BF16)

    def finish(slot, n):
        top = slice(0, n * cap)
        whole(rs.at[slot, hl - 1, 0, top], l_recv.at[slot, hl - 1]).wait()
        give(slot, n, part[slot, 0, top].astype(F32) + rs[slot, hl - 1, 0, top].astype(F32)
             + rs[slot, hs - 1, 1, top].astype(F32))
        if n == 4:
            for j in range(4):
                ret_copy(slot, j, dev(z + (-1, 1)[j % 2] * (slot + 1), (c, 1 - c)[j // 2])).start()
        else:
            ret_copy(slot, 1, partner).start()
            results[e] = ret[slot, 0]

    def finish_last():
        whole(direct, t_recv.at[0]).wait()
        value = part[last, 0, 0:2 * cap].astype(F32)
        for q in range(tp - 1):
            value = value + direct[q].astype(F32)
        give(last, 2, value)
        ret_copy(last, 0, dev(z + steps, c)).start()
        ret_copy(last, 1, dev(z + steps, 1 - c)).start()

    def at(turn, behind, act):
        @pl.when((turn >= behind) & (turn - behind < last))
        def _():
            act(turn - behind, 4)

        @pl.when(turn - behind == -1)
        def _():
            act(mine, 2)

    def turn(t, carry):
        arrive(t, 0)

        @pl.when((t >= 1) & (t <= last))
        def _():
            pick(t - 1, 4)

        @pl.when(t == steps)
        def _():
            pick(last, 2)

        arrive(t, 1)
        arrive(t, 2)
        at(t, hl + 1, finish)
        for h in range(hl - 1, 0, -1):
            at(t, h + 1, functools.partial(hop, h=h))
        at(t, 1, compute)

        @pl.when(t == steps)
        def _():
            compute(last, 2, False)

        return carry

    pick(mine, 2)
    lax.fori_loop(0, last + hl + 1, turn, 0)
    finish_last()

    whole(results.at[0:ep - 1], r_recv.at[0]).wait()
    got = results[...].astype(F32).reshape(ep * cap, share).astype(BF16)
    combined = jnp.dot(c_hi[...], got, preferred_element_type=F32) + jnp.dot(
        c_lo[...], got, preferred_element_type=F32)
    own_sq = jnp.sum(combined * combined, axis=1, keepdims=True)
    eye = lax.broadcasted_iota(I32, (blk, blk), 0) == lax.broadcasted_iota(I32, (blk, blk), 1)
    flat = jnp.sum(jnp.where(eye, jnp.broadcast_to(own_sq, (blk, blk)), 0.0), axis=0, keepdims=True)
    squares[x] = jnp.broadcast_to(jnp.concatenate([flat, flat], axis=1), squares.shape[1:])

    def q_copy(q):
        return pltpu.make_async_remote_copy(
            squares.at[x], squares.at[x], out_sem.at[8], q_recv.at[0],
            device_id={"tp": wrap(x + q, tp)}, device_id_type=MESH)

    for q in range(1, tp):
        q_copy(q).start()

    def amount(units, most):
        b = max(d for d in range(1, most + 1) if units % d == 0)
        return units // b, b

    a, b = amount(2 * steps - 1, 4)
    whole(tok.at[0:a, :, 0:b * blk, :], out_sem.at[0]).wait()
    whole(tab.at[0:a, 0:b], out_sem.at[1]).wait()
    a, b = amount(2 * steps, 4)
    whole(tok.at[0:a, :, 0:b * blk, :], out_sem.at[2]).wait()
    whole(tab.at[0:a, 0:b], out_sem.at[3]).wait()
    if XS:
        whole(rows.at[0:steps, :, 0:XS * share], out_sem.at[4]).wait()
    a, b = amount((4 * last + 2) * cap // 16, 4 * cap // 16)
    whole(part.at[0:a, 0:tp - 1, 0:b * 16], out_sem.at[5]).wait()
    whole(direct, out_sem.at[6]).wait()
    whole(results.at[0:ep - 1], out_sem.at[7]).wait()
    whole(squares.at[0:tp - 1], out_sem.at[8]).wait()
    whole(squares.at[0:tp - 1], q_recv.at[0]).wait()
    everyone = jnp.sum(squares[...], axis=0)[0:1, 0:blk]
    column = jnp.sum(jnp.where(eye, jnp.broadcast_to(everyone, (blk, blk)), 0.0), axis=1, keepdims=True)
    scale = lax.rsqrt(column / (tp * share) + EPS)
    out[...] = (combined * scale * final_in[...]).astype(out.dtype)


def solution(mesh):
    ep, tp = mesh.shape["ep"], mesh.shape["tp"]

    def per_device(tokens, norm_gain, routes, route_weights, w_gate, w_up, w_down, final_gain):
        blk, features = tokens.shape
        cap = max(2, min(blk, 2 * blk * TOP_K // ep))
        share = features // tp
        slots = ep // CORES // 2 + 1
        hl = tp // 2
        zs = tp - XS
        dma = pltpu.SemaphoreType.DMA
        vmem = pltpu.VMEM
        return pl.pallas_call(
            functools.partial(kernel, ep, tp, cap),
            out_shape=jax.ShapeDtypeStruct((blk, share), BF16),
            in_specs=[pl.BlockSpec(memory_space=pl.ANY)] * 8,
            out_specs=pl.BlockSpec(memory_space=pltpu.VMEM),
            scratch_shapes=[
                vmem((slots, zs, 4 * blk, share), BF16),
                vmem((slots, 4, ep, 2 * blk), BF16),
                vmem((slots, 4 * cap, features), BF16),
                vmem((slots, tp, 4 * cap, share), BF16),
                vmem((slots, hl, 2, 4 * cap, share), BF16),
                vmem((tp - 1, 2 * cap, share), BF16),
                vmem((slots, 4, cap, share), BF16),
                vmem((ep, cap, share), BF16),
                vmem((tp, 8, 2 * blk), F32),
                vmem((tp, blk, share), BF16),
                vmem((tp, 1, share), F32),
                vmem((TOP_K, blk), I32),
                vmem((TOP_K, blk), F32),
                vmem((features, 2 * share), BF16),
                vmem((tp, share, share), BF16),
                vmem((1, share), F32),
                vmem((blk, ep * cap), BF16),
                vmem((blk, ep * cap), BF16),
                dma((7,)), dma((9,)),
                dma((slots - 1, 3)), dma((slots, 2)), dma((slots,)), dma((slots, hl)), dma((1,)), dma((1,)), dma((1,)),
            ],
            compiler_params=pltpu.CompilerParams(
                collective_id=0, has_side_effects=True, vmem_limit_bytes=56 * 1024 * 1024),
        )(tokens, norm_gain.reshape(1, features), routes.T, route_weights.T, w_gate, w_up, w_down,
          final_gain.reshape(1, share))

    placed = (
        P(("grp", "ep"), None),
        P(),
        P(("grp", "ep"), None),
        P(("grp", "ep"), None),
        P("ep", None, "tp"),
        P("ep", None, "tp"),
        P("ep", "tp", None),
        P("tp"),
    )
    return jax.shard_map(
        per_device, mesh=mesh, in_specs=placed, out_specs=P(("grp", "ep"), "tp"), check_vma=False
    )
```

time: 125 us -> 121 us (0.968)
  Pallas kernels: 123 us -> 119 us
    pallas_call x1, Pallas kernels: 123 us -> 119 us  [per_device(): pl.pallas_call(functools.partial(kernel, ep, tp, cap), out_shape=jax.Shap...]
where the time goes in v3:
time: 121 us
  Pallas kernels  119 us (98%)
  local copies, waits for them, and re-layouts  1.38 us (1%)
    pallas_call x1, Pallas kernels, per_device(): pl.pallas_call(functools.partial(kernel, ep, tp, cap), out_shape=jax.Shap...  119 us

profile of v3, /device:TPU:65, one launch (start us, length us, event | category | flops | bytes accessed | tf_op | source)
XLA Modules:
  0.0 120.8 jit_solution(17403076808805204474)
XLA Ops:
  0.0 119.4 %shard_map.82 = bf16[64,256]{1,0:T(8,128)(2,1)} custom-call(bf16[64,2048]{1,0:T(8,128)(2,1)} %tokens.1, f32[1,2048]{1,0:T(1,128)} %bitcast.4, s32[6,64]{1,0:T(8,128)} %bitcast.5, f32[6,64]{1,0:T(8,128)} %bitcast.6, bf16[1,2048,256]{2,1,0:T(8,128)(2,1)} %w_gate.1, bf16[1,2048,256]{2,1,0:T(8,128)(2,1)} %w_up.1, bf16[1,256,2048]{2,1,0:T(8,128)(2,1)} %w_down.1, ...), custom_call_target="tpu_custom_call" | custom-call | tf_op jit(solution)/shard_map/pallas_call | solution.py:408
  119.4 1.4 %copy.10 = bf16[64,256]{1,0:T(8,128)(2,1)} copy(bf16[64,256]{1,0:T(8,128)(2,1)} %shard_map.82) | data formatting | bytes 65536

commit v4 on v3

--- a/solution.py
+++ b/solution.py
@@ -13,6 +13,19 @@
 BF16, F32, I32 = jnp.bfloat16, jnp.float32, jnp.int32
 CORES = 2
 XS = 2
+PIECES = (2, 2, 2)
+Z, PICK, COMP, HOP, FIN = range(5)
+ORDER = (
+    (PICK, -1), (Z, 0, 0), (COMP, -1), (Z, 0, 1), (Z, 0, 2), (PICK, 0), (Z, 1, 0), (HOP, -1, 1), (Z, 1, 1),
+    (Z, 1, 2), (COMP, 0), (Z, 2, 0), (PICK, 1), (HOP, -1, 2), (Z, 2, 1), (Z, 2, 2), (HOP, 0, 1), (PICK, 2),
+    (Z, 3, 0), (COMP, 1), (HOP, -1, 3), (Z, 3, 1), (Z, 3, 2), (HOP, 0, 2), (PICK, 3), (Z, 4, 0), (COMP, 2),
+    (FIN, -1), (Z, 4, 1), (HOP, 1, 1), (HOP, 0, 3), (Z, 4, 2), (COMP, 3), (Z, 5, 0), (PICK, 4), (HOP, 2, 1),
+    (Z, 5, 1), (HOP, 1, 2), (FIN, 0), (Z, 5, 2), (HOP, 3, 1), (PICK, 5), (Z, 6, 0), (COMP, 4), (HOP, 2, 2),
+    (Z, 6, 1), (HOP, 1, 3), (Z, 6, 2), (HOP, 3, 2), (Z, 7, 0), (PICK, 6), (COMP, 5), (Z, 7, 1), (HOP, 4, 1),
+    (Z, 7, 2), (HOP, 2, 3), (FIN, 1), (PICK, 7), (HOP, 3, 3), (COMP, 6), (HOP, 5, 1), (HOP, 4, 2), (FIN, 2),
+    (COMP, 7), (FIN, 3), (HOP, 6, 1), (HOP, 5, 2), (HOP, 4, 3), (HOP, 7, 1), (HOP, 6, 2), (HOP, 5, 3), (FIN, 4),
+    (HOP, 7, 2), (HOP, 6, 3), (FIN, 5), (HOP, 7, 3), (FIN, 6), (FIN, 7),
+)
 
 
 def wrap(value, count):
@@ -23,9 +36,9 @@
     ep, tp, cap,
     tokens, norm_gain, routes, route_weights, w_gate, w_up, w_down, final_gain,
     out,
-    tok, tab, rows, part, rs, direct, ret, results, squares,
+    tok, tab, rows, part, rs, ret, results, squares,
     tok_in, gain_in, routes_in, weights_in, wgu, wd, final_in, c_hi, c_lo,
-    in_sem, out_sem, z_recv, d_recv, x_recv, l_recv, t_recv, r_recv, q_recv,
+    in_sem, out_sem, z_recv, d_recv, x_recv, l_recv, r_recv, q_recv,
 ):
     e = lax.axis_index("ep")
     x = lax.axis_index("tp")
@@ -38,7 +51,8 @@
     blk = tok_in.shape[1]
     share = tok_in.shape[2]
     last, mine = steps - 1, steps
-    half = zs // 2
+    cuts = [sum(PIECES[:p]) for p in range(len(PIECES) + 1)]
+    np_ = len(PIECES)
 
     def dev(zz, cc):
         return wrap(zz, nz) * CORES + cc
@@ -74,15 +88,15 @@
         return pltpu.make_async_copy(ref, ref, sem)
 
     near, far = slice(0, blk), slice(blk, 2 * blk)
-    halves = (slice(0, half), slice(half, zs))
+    halves = [slice(a, b) for a, b in zip(cuts, cuts[1:])]
 
     def z_copy(dst_slot, piece, to, src_slot, src_tok, src_tab, dst_tok, dst_tab):
-        if piece < 2:
+        if piece < np_:
             src, dst = tok.at[src_slot, halves[piece], src_tok, :], tok.at[dst_slot, halves[piece], dst_tok, :]
         else:
             src, dst = tab.at[src_slot, src_tab], tab.at[dst_slot, dst_tab]
         return pltpu.make_async_remote_copy(
-            src, dst, out_sem.at[piece // 2], z_recv.at[dst_slot, piece],
+            src, dst, out_sem.at[piece // np_], z_recv.at[dst_slot, piece],
             device_id={"ep": to}, device_id_type=MESH)
 
     def z_own(way, piece):
@@ -97,18 +111,18 @@
         return z_copy(last, piece, jnp.where(c == 0, up_z, down_z), last - 1, there, c, near, 0)
 
     def z_done(slot, piece, n):
-        ref = tok.at[slot, halves[piece], 0:n * blk, :] if piece < 2 else tab.at[slot, 0:n]
+        ref = tok.at[slot, halves[piece], 0:n * blk, :] if piece < np_ else tab.at[slot, 0:n]
         return whole(ref, z_recv.at[slot, piece])
 
     def d_copy(slot, piece, n):
         h = n // 2
-        if piece < 2:
+        if piece < np_:
             src = tok.at[slot, halves[piece], 0:h * blk, :]
             dst = tok.at[slot, halves[piece], h * blk:n * blk, :]
         else:
             src, dst = tab.at[slot, 0:h], tab.at[slot, h:n]
         return pltpu.make_async_remote_copy(
-            src, dst, out_sem.at[2 + piece // 2], d_recv.at[slot, piece // 2],
+            src, dst, out_sem.at[2 + piece // np_], d_recv.at[slot, piece // np_],
             device_id={"ep": partner}, device_id_type=MESH)
 
     def d_done(slot, n):
@@ -133,11 +147,6 @@
         return pltpu.make_async_remote_copy(
             src, rs.at[slot, hop - 1, side, top], out_sem.at[5], l_recv.at[slot, hop - 1],
             device_id={"tp": (x_long, x_short)[side]}, device_id_type=MESH)
-
-    def direct_copy(q):
-        return pltpu.make_async_remote_copy(
-            part.at[last, q, 0:2 * cap], direct.at[tp - q - 1], out_sem.at[6], t_recv.at[0],
-            device_id={"tp": wrap(x + q * dl, tp)}, device_id_type=MESH)
 
     def ret_copy(slot, j, to):
         return pltpu.make_async_remote_copy(
@@ -156,17 +165,15 @@
         value = tok_in[q].astype(F32) * inverse * gain_in[q]
         tok[mine, q, near, :] = value.astype(BF16)
 
-    for q in range(half):
-        norm(q)
-    pl.semaphore_wait(barrier, 5)
-    z_own(0, 0).start()
-    z_own(1, 0).start()
-    for q in range(half, zs):
-        norm(q)
-    z_own(0, 1).start()
-    z_own(1, 1).start()
-    d_copy(mine, 0, 2).start()
-    d_copy(mine, 1, 2).start()
+    for p in range(np_):
+        for q in range(cuts[p], cuts[p + 1]):
+            norm(q)
+        if p == 0:
+            pl.semaphore_wait(barrier, 5)
+        z_own(0, p).start()
+        z_own(1, p).start()
+    for p in range(np_):
+        d_copy(mine, p, 2).start()
 
     for copy in second:
         copy.wait()
@@ -186,9 +193,9 @@
     slots = jnp.dot(hits_b, same, preferred_element_type=F32) * (
         jnp.dot(hits_b, earlier, preferred_element_type=F32) + 1.0)
     tab[mine, 0] = slots.astype(BF16)
-    z_own(0, 2).start()
-    z_own(1, 2).start()
-    d_copy(mine, 2, 2).start()
+    z_own(0, np_).start()
+    z_own(1, np_).start()
+    d_copy(mine, np_, 2).start()
 
     over = (((0,), (0,)), ((), ()))
     slot1 = slots[:, 0:blk].astype(BF16)
@@ -209,25 +216,14 @@
     whole(wd, in_sem.at[6]).wait()
 
     def arrive(slot, piece):
-        @pl.when(slot < last)
-        def _():
-            z_done(slot, piece, 2).wait()
-
-            @pl.when(slot < last - 1)
-            def _():
-                z_next(slot, 0, piece).start()
-                z_next(slot, 1, piece).start()
-
-            @pl.when(slot == last - 1)
-            def _():
-                z_end(piece).start()
-
-            d_copy(slot, piece, 4).start()
-
-        @pl.when(slot == last)
-        def _():
-            z_done(slot, piece, 1).wait()
-            d_copy(slot, piece, 2).start()
+        n = 4 if slot < last else 2
+        z_done(slot, piece, n // 2).wait()
+        if slot < last - 1:
+            z_next(slot, 0, piece).start()
+            z_next(slot, 1, piece).start()
+        elif slot == last - 1:
+            z_end(piece).start()
+        d_copy(slot, piece, n).start()
 
     left_half = lax.broadcasted_iota(I32, (1, 2 * blk), 1) < blk
     my_expert = lax.broadcasted_iota(I32, (ep, 2 * blk), 0) == e
@@ -260,21 +256,16 @@
             if q not in early:
                 one(q)
 
-    def compute(slot, n, ring=True):
-        if XS:
-            whole(rows.at[slot, 0:n * cap, zs * share:], x_recv.at[slot]).wait()
+    def compute(slot, n):
+        whole(rows.at[slot, 0:n * cap, zs * share:], x_recv.at[slot]).wait()
         acc = jnp.dot(rows[slot, 0:n * cap, :], wgu[...], preferred_element_type=F32)
         gate, up = acc[:, :share], acc[:, share:]
         hidden = (gate / (1.0 + jnp.exp(-gate)) * up).astype(BF16)
-        order = sorted(range(tp), key=lambda q: -min(q, tp - q))
-        if ring:
-            order = [hl, tp - hs] + [q for q in order if q not in (hl, tp - hs)]
+        order = [hl, tp - hs] + [q for q in range(tp) if q not in (hl, tp - hs)]
         for place, q in enumerate(order):
             part[slot, q, 0:n * cap] = jnp.dot(hidden, wd[q], preferred_element_type=F32).astype(BF16)
-            if ring and place < 2:
+            if place < 2:
                 rs_copy(slot, n, 1, place).start()
-            if not ring and q:
-                direct_copy(q).start()
 
     def hop(slot, n, h):
         top = slice(0, n * cap)
@@ -299,58 +290,25 @@
         whole(rs.at[slot, hl - 1, 0, top], l_recv.at[slot, hl - 1]).wait()
         give(slot, n, part[slot, 0, top].astype(F32) + rs[slot, hl - 1, 0, top].astype(F32)
              + rs[slot, hs - 1, 1, top].astype(F32))
-        if n == 4:
+        if slot == mine:
+            ret_copy(slot, 1, partner).start()
+            results[e] = ret[slot, 0]
+        elif slot == last:
+            ret_copy(slot, 0, dev(z + steps, c)).start()
+            ret_copy(slot, 1, dev(z + steps, 1 - c)).start()
+        else:
             for j in range(4):
                 ret_copy(slot, j, dev(z + (-1, 1)[j % 2] * (slot + 1), (c, 1 - c)[j // 2])).start()
+
+    for kind, chunk, *which in ORDER:
+        slot = chunk if chunk >= 0 else mine
+        n = 2 if slot >= last else 4
+        if kind == Z:
+            arrive(slot, *which)
+            if which[0] == np_ - 1:
+                arrive(slot, np_)
         else:
-            ret_copy(slot, 1, partner).start()
-            results[e] = ret[slot, 0]
-
-    def finish_last():
-        whole(direct, t_recv.at[0]).wait()
-        value = part[last, 0, 0:2 * cap].astype(F32)
-        for q in range(tp - 1):
-            value = value + direct[q].astype(F32)
-        give(last, 2, value)
-        ret_copy(last, 0, dev(z + steps, c)).start()
-        ret_copy(last, 1, dev(z + steps, 1 - c)).start()
-
-    def at(turn, behind, act):
-        @pl.when((turn >= behind) & (turn - behind < last))
-        def _():
-            act(turn - behind, 4)
-
-        @pl.when(turn - behind == -1)
-        def _():
-            act(mine, 2)
-
-    def turn(t, carry):
-        arrive(t, 0)
-
-        @pl.when((t >= 1) & (t <= last))
-        def _():
-            pick(t - 1, 4)
-
-        @pl.when(t == steps)
-        def _():
-            pick(last, 2)
-
-        arrive(t, 1)
-        arrive(t, 2)
-        at(t, hl + 1, finish)
-        for h in range(hl - 1, 0, -1):
-            at(t, h + 1, functools.partial(hop, h=h))
-        at(t, 1, compute)
-
-        @pl.when(t == steps)
-        def _():
-            compute(last, 2, False)
-
-        return carry
-
-    pick(mine, 2)
-    lax.fori_loop(0, last + hl + 1, turn, 0)
-    finish_last()
+            (pick, compute, hop, finish)[kind - PICK](slot, n, *which)
 
     whole(results.at[0:ep - 1], r_recv.at[0]).wait()
     got = results[...].astype(F32).reshape(ep * cap, share).astype(BF16)
@@ -381,9 +339,7 @@
     whole(tab.at[0:a, 0:b], out_sem.at[3]).wait()
     if XS:
         whole(rows.at[0:steps, :, 0:XS * share], out_sem.at[4]).wait()
-    a, b = amount((4 * last + 2) * cap // 16, 4 * cap // 16)
-    whole(part.at[0:a, 0:tp - 1, 0:b * 16], out_sem.at[5]).wait()
-    whole(direct, out_sem.at[6]).wait()
+    whole(part.at[0:steps, 0:tp - 1], out_sem.at[5]).wait()
     whole(results.at[0:ep - 1], out_sem.at[7]).wait()
     whole(squares.at[0:tp - 1], out_sem.at[8]).wait()
     whole(squares.at[0:tp - 1], q_recv.at[0]).wait()
@@ -416,7 +372,6 @@
                 vmem((slots, 4 * cap, features), BF16),
                 vmem((slots, tp, 4 * cap, share), BF16),
                 vmem((slots, hl, 2, 4 * cap, share), BF16),
-                vmem((tp - 1, 2 * cap, share), BF16),
                 vmem((slots, 4, cap, share), BF16),
                 vmem((ep, cap, share), BF16),
                 vmem((tp, 8, 2 * blk), F32),
@@ -430,7 +385,7 @@
                 vmem((blk, ep * cap), BF16),
                 vmem((blk, ep * cap), BF16),
                 dma((7,)), dma((9,)),
-                dma((slots - 1, 3)), dma((slots, 2)), dma((slots,)), dma((slots, hl)), dma((1,)), dma((1,)), dma((1,)),
+                dma((slots - 1, len(PIECES) + 1)), dma((slots, 2)), dma((slots,)), dma((slots, hl)), dma((1,)), dma((1,)),
             ],
             compiler_params=pltpu.CompilerParams(
                 collective_id=0, has_side_effects=True, vmem_limit_bytes=56 * 1024 * 1024),

time: 121 us -> 114 us (0.942)
  Pallas kernels: 119 us -> 113 us
    pallas_call x1, Pallas kernels: 119 us -> 113 us  [per_device(): pl.pallas_call(functools.partial(kernel, ep, tp, cap), out_shape=jax.Shap...]
where the time goes in v4:
time: 114 us
  Pallas kernels  113 us (99%)
  local copies, waits for them, and re-layouts  1.38 us (1%)
    pallas_call x1, Pallas kernels, per_device(): pl.pallas_call(functools.partial(kernel, ep, tp, cap), out_shape=jax.Shap...  113 us

profile of v4, /device:TPU:65, one launch (start us, length us, event | category | flops | bytes accessed | tf_op | source)
XLA Modules:
  0.0 114.1 jit_solution(1649245039355808305)
XLA Ops:
  0.0 112.7 %shard_map.82 = bf16[64,256]{1,0:T(8,128)(2,1)} custom-call(bf16[64,2048]{1,0:T(8,128)(2,1)} %tokens.1, f32[1,2048]{1,0:T(1,128)} %bitcast.4, s32[6,64]{1,0:T(8,128)} %bitcast.5, f32[6,64]{1,0:T(8,128)} %bitcast.6, bf16[1,2048,256]{2,1,0:T(8,128)(2,1)} %w_gate.1, bf16[1,2048,256]{2,1,0:T(8,128)(2,1)} %w_up.1, bf16[1,256,2048]{2,1,0:T(8,128)(2,1)} %w_down.1, ...), custom_call_target="tpu_custom_call" | custom-call | tf_op jit(solution)/shard_map/pallas_call | solution.py:364
  112.7 1.4 %copy.10 = bf16[64,256]{1,0:T(8,128)(2,1)} copy(bf16[64,256]{1,0:T(8,128)(2,1)} %shard_map.82) | data formatting | bytes 65536

commit v5 on v4

--- a/solution.py
+++ b/solution.py
@@ -36,8 +36,8 @@
     ep, tp, cap,
     tokens, norm_gain, routes, route_weights, w_gate, w_up, w_down, final_gain,
     out,
-    tok, tab, rows, part, rs, ret, results, squares,
-    tok_in, gain_in, routes_in, weights_in, wgu, wd, final_in, c_hi, c_lo,
+    tok, tab, rows, part, rs, ret, results, late, squares,
+    tok_in, gain_in, routes_in, weights_in, wgu, wd, final_in, c_hi, c_lo, cl_hi, cl_lo,
     in_sem, out_sem, z_recv, d_recv, x_recv, l_recv, r_recv, q_recv,
 ):
     e = lax.axis_index("ep")
@@ -149,9 +149,9 @@
             device_id={"tp": (x_long, x_short)[side]}, device_id_type=MESH)
 
     def ret_copy(slot, j, to):
+        dst, sem = (late.at[c], r_recv.at[1]) if slot == last else (results.at[e], r_recv.at[0])
         return pltpu.make_async_remote_copy(
-            ret.at[slot, j], results.at[e], out_sem.at[7], r_recv.at[0],
-            device_id={"ep": to}, device_id_type=MESH)
+            ret.at[slot, j], dst, out_sem.at[7], sem, device_id={"ep": to}, device_id_type=MESH)
 
     whole(tok_in, in_sem.at[0]).wait()
     whole(gain_in, in_sem.at[1]).wait()
@@ -199,18 +199,24 @@
 
     over = (((0,), (0,)), ((), ()))
     slot1 = slots[:, 0:blk].astype(BF16)
-    lane = lax.broadcasted_iota(I32, (ep, ep * cap), 1)
-    start = lax.broadcasted_iota(I32, (ep, ep * cap), 0) * cap
-    inside = jnp.where((lane >= start) & (lane < start + cap), 1.0, 0.0)
-    spread = inside.astype(BF16)
-    want = jnp.sum(inside * (lane - start + 1).astype(F32), axis=0, keepdims=True)
     wt_hi = wt.astype(BF16)
     wt_lo = (wt - wt_hi.astype(F32)).astype(BF16)
-    match = lax.dot_general(slot1, spread, over, preferred_element_type=F32) == want
-    c_hi[...] = jnp.where(
-        match, lax.dot_general(wt_hi, spread, over, preferred_element_type=F32), 0.0).astype(BF16)
-    c_lo[...] = jnp.where(
-        match, lax.dot_general(wt_lo, spread, over, preferred_element_type=F32), 0.0).astype(BF16)
+
+    def put_together(first, count, hi, lo):
+        lane = lax.broadcasted_iota(I32, (ep, count * cap), 1)
+        start = (lax.broadcasted_iota(I32, (ep, count * cap), 0) - first) * cap
+        inside = jnp.where((lane >= start) & (lane < start + cap), 1.0, 0.0)
+        spread = inside.astype(BF16)
+        want = jnp.sum(inside * (lane - start + 1).astype(F32), axis=0, keepdims=True)
+        match = lax.dot_general(slot1, spread, over, preferred_element_type=F32) == want
+        for weight, ref in ((wt_hi, hi), (wt_lo, lo)):
+            value = lax.dot_general(weight, spread, over, preferred_element_type=F32)
+            ref[...] = jnp.where(match, value, 0.0).astype(BF16)
+
+    opposite = dev(z + steps, 0)
+    put_together(0, ep, c_hi, c_lo)
+    put_together(opposite, CORES, cl_hi, cl_lo)
+    results[pl.ds(opposite, CORES)] = jnp.zeros((CORES, cap, share), BF16)
 
     whole(wgu, in_sem.at[5]).wait()
     whole(wd, in_sem.at[6]).wait()
@@ -310,10 +316,15 @@
         else:
             (pick, compute, hop, finish)[kind - PICK](slot, n, *which)
 
-    whole(results.at[0:ep - 1], r_recv.at[0]).wait()
-    got = results[...].astype(F32).reshape(ep * cap, share).astype(BF16)
-    combined = jnp.dot(c_hi[...], got, preferred_element_type=F32) + jnp.dot(
-        c_lo[...], got, preferred_element_type=F32)
+    def weigh(ref, hi, lo):
+        got = ref[...].astype(F32).reshape(-1, share).astype(BF16)
+        return jnp.dot(hi[...], got, preferred_element_type=F32) + jnp.dot(
+            lo[...], got, preferred_element_type=F32)
+
+    whole(results.at[0:ep - 1 - CORES], r_recv.at[0]).wait()
+    combined = weigh(results, c_hi, c_lo)
+    whole(late, r_recv.at[1]).wait()
+    combined = combined + weigh(late, cl_hi, cl_lo)
     own_sq = jnp.sum(combined * combined, axis=1, keepdims=True)
     eye = lax.broadcasted_iota(I32, (blk, blk), 0) == lax.broadcasted_iota(I32, (blk, blk), 1)
     flat = jnp.sum(jnp.where(eye, jnp.broadcast_to(own_sq, (blk, blk)), 0.0), axis=0, keepdims=True)
@@ -374,6 +385,7 @@
                 vmem((slots, hl, 2, 4 * cap, share), BF16),
                 vmem((slots, 4, cap, share), BF16),
                 vmem((ep, cap, share), BF16),
+                vmem((CORES, cap, share), BF16),
                 vmem((tp, 8, 2 * blk), F32),
                 vmem((tp, blk, share), BF16),
                 vmem((tp, 1, share), F32),
@@ -384,8 +396,10 @@
                 vmem((1, share), F32),
                 vmem((blk, ep * cap), BF16),
                 vmem((blk, ep * cap), BF16),
+                vmem((blk, CORES * cap), BF16),
+                vmem((blk, CORES * cap), BF16),
                 dma((7,)), dma((9,)),
-                dma((slots - 1, len(PIECES) + 1)), dma((slots, 2)), dma((slots,)), dma((slots, hl)), dma((1,)), dma((1,)),
+                dma((slots - 1, len(PIECES) + 1)), dma((slots, 2)), dma((slots,)), dma((slots, hl)), dma((2,)), dma((1,)),
             ],
             compiler_params=pltpu.CompilerParams(
                 collective_id=0, has_side_effects=True, vmem_limit_bytes=56 * 1024 * 1024),

time: 114 us -> 114 us (level)
  no operation moved by 1% of the time
where the time goes in v5:
time: 114 us
  Pallas kernels  112 us (98%)
  local copies, waits for them, and re-layouts  1.38 us (1%)
    pallas_call x1, Pallas kernels, per_device(): pl.pallas_call(functools.partial(kernel, ep, tp, cap), out_shape=jax.Shap...  112 us

profile of v5, /device:TPU:65, one launch (start us, length us, event | category | flops | bytes accessed | tf_op | source)
XLA Modules:
  0.0 113.9 jit_solution(3674785865553682407)
XLA Ops:
  0.0 112.5 %shard_map.82 = bf16[64,256]{1,0:T(8,128)(2,1)} custom-call(bf16[64,2048]{1,0:T(8,128)(2,1)} %tokens.1, f32[1,2048]{1,0:T(1,128)} %bitcast.4, s32[6,64]{1,0:T(8,128)} %bitcast.5, f32[6,64]{1,0:T(8,128)} %bitcast.6, bf16[1,2048,256]{2,1,0:T(8,128)(2,1)} %w_gate.1, bf16[1,2048,256]{2,1,0:T(8,128)(2,1)} %w_up.1, bf16[1,256,2048]{2,1,0:T(8,128)(2,1)} %w_down.1, ...), custom_call_target="tpu_custom_call" | custom-call | tf_op jit(solution)/shard_map/pallas_call | solution.py:375
  112.5 1.4 %copy.10 = bf16[64,256]{1,0:T(8,128)(2,1)} copy(bf16[64,256]{1,0:T(8,128)(2,1)} %shard_map.82) | data formatting | bytes 65536
